TPU v7x, 32 devices: a whole 2x2x4 slice. The times are simulated.
32 devices in a mesh: ep: 8 (over z, core), tp: 4 (over y, x).
Axes of the slice: x: 2, y: 2, z: 4, core: 2. Of those that a mesh axis runs over, the one named last changes fastest.
Arguments:
- tokens: bfloat16 [512, 2048], P('ep', 'tp'), may hold values from -6 to 6
- gain_mix: float32 [2048], replicated, may hold values from 0.1 to 1.9
- w_in: bfloat16 [2048, 1024], P(None, 'tp'), may hold values from -0.125 to 0.125
- decay_rate: float32 [64, 64], P('tp'), may hold values from 0.05 to 3
- frequency: float32 [64, 64], P('tp'), may hold values from -3 to 3
- log_step: float32 [64], P('tp'), may hold values from -3 to 0
- input_real: float32 [64, 64, 16], P('tp'), may hold values from -1 to 1
- input_imag: float32 [64, 64, 16], P('tp'), may hold values from -1 to 1
- readout_real: float32 [64, 16, 64], P('tp'), may hold values from -0.75 to 0.75
- readout_imaginary: float32 [64, 16, 64], P('tp'), may hold values from -0.75 to 0.75
- passthrough_scale: float32 [1024], P('tp'), may hold values from -4 to 4
- state_real: float32 [512, 64, 64], P('ep', 'tp'), may hold values from -4 to 4
- state_imag: float32 [512, 64, 64], P('ep', 'tp'), may hold values from -4 to 4
- w_out: bfloat16 [1024, 2048], replicated, may hold values from -0.1875 to 0.1875
- gain_ffn: float32 [2048], replicated, may hold values from 0.1 to 1.9
- expert_choice: int32 [512, 2], P('ep'), may hold values from 0 to 7, all different within a row; in each aligned block of 64 rows (0 to 63, 64 to 127, ...) at most 32 rows name the same one
- expert_weight: float32 [512, 2], P('ep'), may hold values from 0.2 to 1
- w_gate: bfloat16 [8, 2048, 8192], P('ep', None, 'tp'), may hold values from -0.125 to 0.125
- w_up: bfloat16 [8, 2048, 8192], P('ep', None, 'tp'), may hold values from -0.125 to 0.125
- w_down: bfloat16 [8, 8192, 2048], P('ep', 'tp'), may hold values from -0.0625 to 0.0625
Outputs:
- layer_out: bfloat16 [512, 2048], P('ep', 'tp')
- next_state_real: float32 [512, 64, 64], P('ep', 'tp')
- next_state_imaginary: float32 [512, 64, 64], P('ep', 'tp')
Inputs may be any that keep to these rules, and one draw needn't show every extreme that they name: `expert_choice`: each row names 2 different experts; in the rows of one index of ep (aligned blocks of 64 rows) no expert is named more than 32 times, a bound that some block reaches.
All inputs are finite; a program needn't handle non-finite values.
Results may differ from a plain program's by a relative error of at most 0.017.
Values may be sent and summed in bfloat16 or wider, within the bound.
A program may use at most 64 MiB of HBM per device.

v0:
```python
import functools

import jax
import jax.numpy as jnp
from jax import lax
from jax.experimental import pallas as pl
from jax.experimental.pallas import tpu as pltpu
from jax.sharding import PartitionSpec as P


def state_step(
    drive,
    real_state,
    imag_state,
    decay_rate,
    frequency,
    log_step,
    input_real,
    input_imag,
    readout_real,
    readout_imaginary,
    passthrough_scale,
):
    highest_precision = lax.Precision.HIGHEST
    count_of_groups, count_of_channels = (input_real.shape[0], input_real.shape[2])
    step = jnp.exp(log_step)[:, None]
    lam_real = -decay_rate
    magnitude = jnp.exp(lam_real * step)
    abar_real = magnitude * jnp.cos(frequency * step)
    abar_imag = magnitude * jnp.sin(frequency * step)
    denom = lam_real * lam_real + frequency * frequency
    numer = abar_real - 1.0
    factor_real = (numer * lam_real + abar_imag * frequency) / denom
    factor_imag = (abar_imag * lam_real - numer * frequency) / denom
    bbar_real = factor_real[..., None] * input_real - factor_imag[..., None] * input_imag
    bbar_imag = factor_real[..., None] * input_imag + factor_imag[..., None] * input_real
    float_values = drive.astype(jnp.float32).reshape(
        drive.shape[0], count_of_groups, count_of_channels
    )
    push_real = jnp.einsum("sgc,gpc->sgp", float_values, bbar_real, precision=highest_precision)
    push_imag = jnp.einsum("sgc,gpc->sgp", float_values, bbar_imag, precision=highest_precision)
    next_state_real = abar_real * real_state - abar_imag * imag_state + push_real
    next_state_imaginary = abar_real * imag_state + abar_imag * real_state + push_imag
    readout_matrix = (
        jnp.einsum("jdr,dyr->jdy", next_state_real, readout_real, precision=highest_precision)
        - jnp.einsum(
            "jdr,dyr->jdy", next_state_imaginary, readout_imaginary, precision=highest_precision
        )
        + passthrough_scale.reshape(count_of_groups, count_of_channels) * float_values
    )
    mixer = jax.nn.gelu(
        readout_matrix.reshape(drive.shape[0], count_of_groups * count_of_channels)
    ).astype(jnp.bfloat16)
    return (mixer, next_state_real, next_state_imaginary)


def slot_table(routes, expert_count, capacity):
    flat = routes.reshape(-1)
    onehot = (flat[:, None] == jnp.arange(expert_count, dtype=jnp.int32)[None, :]).astype(jnp.int32)
    before = jnp.cumsum(onehot, axis=0) - onehot
    slot = jnp.sum(before * onehot, axis=1)
    target = flat * capacity + slot
    return (
        target[None, :] == jnp.arange(expert_count * capacity, dtype=jnp.int32)[:, None]
    ).astype(jnp.bfloat16)


def flipped(index, mask, count):
    other = 0
    bit = 1
    while bit < count:
        digit = lax.rem(lax.div(index, bit), 2)
        other = other + bit * ((1 - digit) if mask & bit else digit)
        bit *= 2
    return other


def expert_kernel(
    ep_count,
    tp_count,
    mixer_ref,
    tokens_ref,
    gain_ref,
    choice_ref,
    weight_ref,
    out_w_hbm,
    gate_hbm,
    up_hbm,
    down_hbm,
    out_ref,
    mixers,
    out_w,
    after_buffer,
    gate_w,
    up_w,
    down_w,
    outgoing,
    arrived,
    gate_sum,
    up_sum,
    hidden,
    parts,
    parts_in,
    results,
    returned,
    mix_send,
    mix_recv,
    weight_sem,
    out_send,
    out_recv,
    near_send,
    near_recv,
    far_send,
    far_recv,
    part_send,
    part_recv,
    back_send,
    back_recv,
):
    me_ep, me_tp = lax.axis_index("ep"), lax.axis_index("tp")
    capacity, width = outgoing.shape[1], outgoing.shape[2]
    half = ep_count // 2
    peers = sorted(range(1, tp_count), key=lambda p: (bin(p).count("1"), p))
    near = [p for p in peers if bin(p).count("1") == 1]
    far = [p for p in peers if p not in near]
    tp_of = {p: flipped(me_tp, p, tp_count) for p in range(tp_count)}
    ep_of = {j: flipped(me_ep, j, ep_count) for j in range(ep_count)}

    def remote(src, dst, send, recv, **where):
        return pltpu.make_async_remote_copy(
            src_ref=src,
            dst_ref=dst,
            send_sem=send,
            recv_sem=recv,
            device_id=where,
            device_id_type=pl.DeviceIdType.MESH,
        )

    order = [0] + peers
    loads = {}
    channels = mixer_ref.shape[1]
    for p in order:
        rows = pl.ds(pl.multiple_of(tp_of[p] * channels, channels), channels)
        loads[3, p] = pltpu.make_async_copy(out_w_hbm.at[rows], out_w.at[p], weight_sem.at[3, p])
        loads[3, p].start()
    for p in order:
        rows = pl.ds(pl.multiple_of(tp_of[p] * width, width), width)
        loads[0, p] = pltpu.make_async_copy(gate_hbm.at[0, rows], gate_w.at[p], weight_sem.at[0, p])
        loads[1, p] = pltpu.make_async_copy(up_hbm.at[0, rows], up_w.at[p], weight_sem.at[1, p])
        loads[0, p].start()
        loads[1, p].start()
    down_order = far + near + [0]
    for p in down_order:
        columns = pl.ds(pl.multiple_of(tp_of[p] * width, width), width)
        loads[2, p] = pltpu.make_async_copy(
            down_hbm.at[0, :, columns], down_w.at[p], weight_sem.at[2, p]
        )
        loads[2, p].start()

    barrier = pltpu.get_barrier_semaphore()
    for p in peers:
        pl.semaphore_signal(
            barrier, inc=1, device_id={"tp": tp_of[p]}, device_id_type=pl.DeviceIdType.MESH
        )
    for j in range(1, ep_count):
        pl.semaphore_signal(
            barrier, inc=1, device_id={"ep": ep_of[j]}, device_id_type=pl.DeviceIdType.MESH
        )
    mixers[0] = mixer_ref[...]
    pl.semaphore_wait(barrier, len(peers) + ep_count - 1)
    mix_copies = {}
    for p in far + near:
        mix_copies[p] = remote(
            mixer_ref, mixers.at[p], mix_send.at[p], mix_recv.at[p], tp=tp_of[p]
        )
        mix_copies[p].start()

    row_count, top_count = choice_ref.shape
    choice, weight = choice_ref[...], weight_ref[...]
    spots = lax.broadcasted_iota(jnp.int32, (row_count, ep_count * capacity), 1)
    names = lax.broadcasted_iota(jnp.int32, (row_count, 128), 1)
    picks = [(choice[:, k : k + 1] == names).astype(jnp.float32) for k in range(top_count)]
    earlier = (
        lax.broadcasted_iota(jnp.int32, (row_count, row_count), 1)
        < lax.broadcasted_iota(jnp.int32, (row_count, row_count), 0)
    ).astype(jnp.float32)
    before = jnp.dot(
        earlier.astype(jnp.bfloat16),
        sum(picks).astype(jnp.bfloat16),
        preferred_element_type=jnp.float32,
    )
    table, weights = 0.0, 0.0
    for k in range(top_count):
        slot = jnp.sum(before * picks[k], axis=1, keepdims=True).astype(jnp.int32)
        hit = (choice[:, k : k + 1] * capacity + slot == spots).astype(jnp.float32)
        table = table + hit
        weights = weights + hit * weight[:, k : k + 1]
        before = before + picks[k]
    high = weights.astype(jnp.bfloat16)
    low = (weights - high.astype(jnp.float32)).astype(jnp.bfloat16)

    mixed = None
    for p in order:
        loads[3, p].wait()
        if p:
            mix_copies[p].wait_recv()
        term = jnp.dot(mixers[p], out_w[p], preferred_element_type=jnp.float32)
        mixed = term if mixed is None else mixed + term
    mixed = mixed.astype(jnp.bfloat16).astype(jnp.float32)
    after = (tokens_ref[...].astype(jnp.float32) + mixed).astype(jnp.bfloat16).astype(jnp.float32)
    scale = lax.rsqrt(jnp.mean(after * after, axis=1, keepdims=True) + 1e-06)
    after_buffer[...] = after
    own = pl.ds(pl.multiple_of(me_tp * width, width), width)
    normed = (after_buffer[:, own] * scale * gain_ref[:, own]).astype(jnp.bfloat16)
    sent = jnp.dot(table.T.astype(jnp.bfloat16), normed, preferred_element_type=jnp.float32)
    outgoing[...] = sent.astype(jnp.bfloat16).reshape(outgoing.shape)
    arrived[0, 0] = outgoing[me_ep]

    out_copies = {}
    for j in range(1, ep_count):
        out_copies[j] = remote(
            outgoing.at[ep_of[j]], arrived.at[0, j], out_send.at[j], out_recv.at[j], ep=ep_of[j]
        )
        out_copies[j].start()
    near_copies, far_copies = {}, {}
    for part in range(2):
        for j in range(part * half, part * half + half):
            if j:
                out_copies[j].wait_recv()
            for p in near:
                near_copies[p, j] = remote(
                    arrived.at[0, j],
                    arrived.at[p, j],
                    near_send.at[p, j],
                    near_recv.at[p, j],
                    tp=tp_of[p],
                )
                near_copies[p, j].start()
        for p in far:
            blocks = pl.ds(part * half, half)
            far_copies[p, part] = remote(
                arrived.at[0, blocks],
                arrived.at[p, blocks],
                far_send.at[p, part],
                far_recv.at[p, part],
                tp=tp_of[p],
            )
            far_copies[p, part].start()

    rows = ep_count * capacity
    hidden_width = hidden.shape[1]
    tile = next(t for t in (512, 256, 128) if hidden_width % t == 0)
    for place, p in enumerate(order):
        if p in near:
            for j in range(ep_count):
                near_copies[p, j].wait_recv()
        elif p:
            for part in range(2):
                far_copies[p, part].wait_recv()
        loads[0, p].wait()
        loads[1, p].wait()

        @pl.loop(0, hidden_width // tile)
        def _(n, place=place, p=p):
            columns = pl.ds(pl.multiple_of(n * tile, tile), tile)
            block = arrived[p].reshape(rows, width)
            gate = jnp.dot(block, gate_w[p, :, columns], preferred_element_type=jnp.float32)
            upper = jnp.dot(block, up_w[p, :, columns], preferred_element_type=jnp.float32)
            if place:
                gate = gate + gate_sum[:, columns]
                upper = upper + up_sum[:, columns]
            if place == len(order) - 1:
                hidden[:, columns] = (jax.nn.silu(gate) * upper).astype(jnp.bfloat16)
            else:
                gate_sum[:, columns] = gate
                up_sum[:, columns] = upper

    def part_copy(p, part):
        blocks = pl.ds((1 - part) * half * capacity, half * capacity)
        return remote(
            parts.at[p, blocks],
            parts_in.at[p, blocks],
            part_send.at[p, part],
            part_recv.at[p, part],
            tp=tp_of[p],
        )

    part_copies = {(p, part): part_copy(p, part) for p in peers for part in range(2)}
    cut = next(t for t in (256, 128) if width % t == 0)
    for p in down_order:
        loads[2, p].wait()

        @pl.loop(0, width // cut)
        def _(n, p=p):
            columns = pl.ds(pl.multiple_of(n * cut, cut), cut)
            parts[p, :, columns] = jnp.dot(
                hidden[...], down_w[p, :, columns], preferred_element_type=jnp.float32
            ).astype(jnp.bfloat16)

        if p:
            part_copies[p, 0].start()
        if p == down_order[-2]:
            for q in down_order[:-1]:
                part_copies[q, 1].start()

    back_copies = {}
    for part in range(2):
        blocks = pl.ds((1 - part) * half * capacity, half * capacity)
        total = None
        for p in range(tp_count):
            if p:
                part_copies[p, part].wait_recv()
                piece = parts_in[p, blocks].astype(jnp.float32)
            else:
                piece = parts[0, blocks].astype(jnp.float32)
            total = piece if total is None else total + piece
        first = (1 - part) * half
        results[pl.ds(first, half)] = total.astype(jnp.bfloat16).reshape(half, capacity, width)
        for j in reversed(range(first, first + half)):
            if j:
                back_copies[j] = remote(
                    results.at[j],
                    returned.at[me_ep],
                    back_send.at[j],
                    back_recv.at[j],
                    ep=ep_of[j],
                )
                back_copies[j].start()
    returned[me_ep] = results[0]
    for j in range(1, ep_count):
        remote(
            results.at[j], returned.at[ep_of[j]], back_send.at[j], back_recv.at[j], ep=ep_of[j]
        ).wait_recv()
    everything = returned[...].reshape(rows, width)
    weighted = jnp.dot(high, everything, preferred_element_type=jnp.float32)
    weighted = weighted + jnp.dot(low, everything, preferred_element_type=jnp.float32)
    out_ref[...] = (after_buffer[:, own] + weighted).astype(jnp.bfloat16)
    for copies in (mix_copies, out_copies, near_copies, far_copies, part_copies, back_copies):
        for copy in copies.values():
            copy.wait_send()


def gather_kernel(
    tp_count,
    tokens_ref,
    gain_ref,
    weight_hbm,
    all_ref,
    drive_ref,
    pieces,
    weight,
    load_sem,
    send_sem,
    recv_sem,
):
    me_tp = lax.axis_index("tp")
    width = tokens_ref.shape[1]
    tp_of = {p: flipped(me_tp, p, tp_count) for p in range(tp_count)}
    order = sorted(range(tp_count), key=lambda p: (bin(p).count("1"), p))
    loads, copies = {}, {}
    for p in order:
        rows = pl.ds(pl.multiple_of(tp_of[p] * width, width), width)
        loads[p] = pltpu.make_async_copy(weight_hbm.at[rows], weight.at[p], load_sem.at[p])
        loads[p].start()
    barrier = pltpu.get_barrier_semaphore()
    for p in order[1:]:
        pl.semaphore_signal(
            barrier, inc=1, device_id={"tp": tp_of[p]}, device_id_type=pl.DeviceIdType.MESH
        )
    pl.semaphore_wait(barrier, tp_count - 1)
    for p in order[1:]:
        copies[p] = pltpu.make_async_remote_copy(
            src_ref=tokens_ref,
            dst_ref=pieces.at[p],
            send_sem=send_sem.at[p],
            recv_sem=recv_sem.at[p],
            device_id={"tp": tp_of[p]},
            device_id_type=pl.DeviceIdType.MESH,
        )
        copies[p].start()
    pieces[0] = tokens_ref[...]
    squares = 0.0
    for p in order:
        if p:
            copies[p].wait_recv()
        piece = pieces[p]
        all_ref[:, pl.ds(pl.multiple_of(tp_of[p] * width, width), width)] = piece
        floats = piece.astype(jnp.float32)
        squares = squares + jnp.sum(floats * floats, axis=1, keepdims=True)
    scale = lax.rsqrt(squares / (width * tp_count) + 1e-06)
    drive = None
    for p in order:
        normed = (pieces[p].astype(jnp.float32) * scale * gain_ref[tp_of[p]]).astype(jnp.bfloat16)
        loads[p].wait()
        term = jnp.dot(normed, weight[p], preferred_element_type=jnp.float32)
        drive = term if drive is None else drive + term
    drive_ref[...] = drive.astype(jnp.bfloat16)
    for p in order[1:]:
        copies[p].wait_send()


def gather_call(tokens, gain, w_in, tp_count):
    row_count, width = tokens.shape
    channels = w_in.shape[1]
    dma = pltpu.SemaphoreType.DMA((tp_count,))
    vmem = pl.BlockSpec(memory_space=pltpu.VMEM)
    return pl.pallas_call(
        functools.partial(gather_kernel, tp_count),
        out_shape=(
            jax.ShapeDtypeStruct((row_count, width * tp_count), jnp.bfloat16),
            jax.ShapeDtypeStruct((row_count, channels), jnp.bfloat16),
        ),
        in_specs=[vmem, vmem, pl.BlockSpec(memory_space=pl.ANY)],
        out_specs=(vmem, vmem),
        scratch_shapes=[
            pltpu.VMEM((tp_count, row_count, width), jnp.bfloat16),
            pltpu.VMEM((tp_count, width, channels), jnp.bfloat16),
            dma,
            dma,
            dma,
        ],
        compiler_params=pltpu.CompilerParams(collective_id=1, has_side_effects=True),
    )(tokens, gain.reshape(tp_count, 1, width), w_in)


def expert_call(
    mixer, tokens, gain, choice, weight, w_out, w_gate, w_up, w_down, capacity, ep_count, tp_count
):
    row_count, full_width = tokens.shape
    channels = mixer.shape[1]
    width = full_width // tp_count
    slots = ep_count * capacity
    hidden_width = w_gate.shape[2]
    bf16, f32 = jnp.bfloat16, jnp.float32
    dma = pltpu.SemaphoreType.DMA
    vmem = pl.BlockSpec(memory_space=pltpu.VMEM)
    hbm = pl.BlockSpec(memory_space=pl.ANY)
    return pl.pallas_call(
        functools.partial(expert_kernel, ep_count, tp_count),
        out_shape=jax.ShapeDtypeStruct((row_count, width), bf16),
        in_specs=[vmem] * 5 + [hbm] * 4,
        out_specs=vmem,
        scratch_shapes=[
            pltpu.VMEM((tp_count, row_count, channels), bf16),
            pltpu.VMEM((tp_count, channels, full_width), bf16),
            pltpu.VMEM((row_count, full_width), f32),
            pltpu.VMEM((tp_count, width, hidden_width), bf16),
            pltpu.VMEM((tp_count, width, hidden_width), bf16),
            pltpu.VMEM((tp_count, hidden_width, width), bf16),
            pltpu.VMEM((ep_count, capacity, width), bf16),
            pltpu.VMEM((tp_count, ep_count, capacity, width), bf16),
            pltpu.VMEM((slots, hidden_width), f32),
            pltpu.VMEM((slots, hidden_width), f32),
            pltpu.VMEM((slots, hidden_width), bf16),
            pltpu.VMEM((tp_count, slots, width), bf16),
            pltpu.VMEM((tp_count, slots, width), bf16),
            pltpu.VMEM((ep_count, capacity, width), bf16),
            pltpu.VMEM((ep_count, capacity, width), bf16),
            dma((tp_count,)),
            dma((tp_count,)),
            dma((4, tp_count)),
            dma((ep_count,)),
            dma((ep_count,)),
            dma((tp_count, ep_count)),
            dma((tp_count, ep_count)),
            dma((tp_count, 2)),
            dma((tp_count, 2)),
            dma((tp_count, 2)),
            dma((tp_count, 2)),
            dma((ep_count,)),
            dma((ep_count,)),
        ],
        compiler_params=pltpu.CompilerParams(
            collective_id=0, has_side_effects=True, vmem_limit_bytes=60 * 1024 * 1024
        ),
    )(mixer, tokens, gain.reshape(1, full_width), choice, weight, w_out, w_gate, w_up, w_down)


def plain_experts(normed, after, table, expert_weight, w_gate, w_up, w_down):
    row_count, top_count = expert_weight.shape
    expert_count = lax.axis_size("ep")
    capacity = table.shape[0] // expert_count
    width = normed.shape[1]
    repeated = jnp.repeat(normed, top_count, axis=0)
    sent = jnp.dot(table, repeated, preferred_element_type=jnp.float32).astype(jnp.bfloat16)
    sent = sent.reshape(expert_count, capacity, width)
    arrived = lax.all_to_all(sent, "ep", split_axis=0, concat_axis=0, tiled=True)
    flat = arrived.reshape(expert_count * capacity, width)
    piece = lax.all_gather(flat, "tp", axis=1, tiled=True)
    gate = jnp.dot(piece, w_gate[0], preferred_element_type=jnp.float32)
    upper = jnp.dot(piece, w_up[0], preferred_element_type=jnp.float32)
    hidden = (jax.nn.silu(gate) * upper).astype(jnp.bfloat16)
    partial_value = jnp.dot(hidden, w_down[0], preferred_element_type=jnp.float32)
    summed = lax.psum_scatter(
        partial_value.astype(jnp.bfloat16), "tp", scatter_dimension=1, tiled=True
    )
    results = summed.reshape(expert_count, capacity, width)
    returned = lax.all_to_all(results, "ep", split_axis=0, concat_axis=0, tiled=True)
    returned = returned.reshape(expert_count * capacity, width)
    picked = jnp.dot(table.T, returned, preferred_element_type=jnp.float32)
    picked = picked.reshape(row_count, top_count, width)
    weighted = jnp.sum(picked * expert_weight[..., None], axis=1)
    return (after.astype(jnp.float32) + weighted).astype(jnp.bfloat16)


def norm(values, gains):
    floats = values.astype(jnp.float32)
    scale = lax.rsqrt(jnp.mean(floats * floats, axis=1, keepdims=True) + 1e-06)
    return (floats * scale * gains).astype(jnp.bfloat16)


def power_of_two(count):
    return count & (count - 1) == 0


def body(
    tokens,
    gain_mix,
    w_in,
    decay_rate,
    frequency,
    log_step,
    input_real,
    input_imag,
    readout_real,
    readout_imaginary,
    passthrough_scale,
    state_real,
    state_imag,
    w_out,
    gain_ffn,
    expert_choice,
    expert_weight,
    w_gate,
    w_up,
    w_down,
):
    tp_count = lax.axis_size("tp")
    expert_count = lax.axis_size("ep")
    row_count, local_width = tokens.shape
    feature_start = lax.axis_index("tp") * local_width
    top_count = expert_choice.shape[1]
    capacity = 2 * row_count * top_count // expert_count
    fused = (
        local_width % 128 == 0
        and w_gate.shape[2] % 128 == 0
        and capacity % 16 == 0
        and power_of_two(tp_count)
        and power_of_two(expert_count)
        and 2 < tp_count <= 8
        and 1 < expert_count <= 8
        and w_in.shape[1] % 128 == 0
        and row_count % 16 == 0
    )
    if fused:
        all_tokens, drive = gather_call(tokens, gain_mix, w_in, tp_count)
    else:
        all_tokens = lax.all_gather(tokens, "tp", axis=1, tiled=True)
        drive = jnp.dot(
            norm(all_tokens, gain_mix), w_in, preferred_element_type=jnp.float32
        ).astype(jnp.bfloat16)
    mixer, next_state_real, next_state_imaginary = state_step(
        drive,
        state_real,
        state_imag,
        decay_rate,
        frequency,
        log_step,
        input_real,
        input_imag,
        readout_real,
        readout_imaginary,
        passthrough_scale,
    )
    if fused:
        layer_out = expert_call(
            mixer,
            all_tokens,
            gain_ffn,
            expert_choice,
            expert_weight,
            w_out,
            w_gate,
            w_up,
            w_down,
            capacity,
            expert_count,
            tp_count,
        )
        return (layer_out, next_state_real, next_state_imaginary)
    table = slot_table(expert_choice, expert_count, capacity)
    mixed = jnp.dot(
        lax.all_gather(mixer, "tp", axis=1, tiled=True), w_out, preferred_element_type=jnp.float32
    ).astype(jnp.bfloat16)
    after_all = (all_tokens.astype(jnp.float32) + mixed.astype(jnp.float32)).astype(jnp.bfloat16)
    normed_all = norm(after_all, gain_ffn)
    after = lax.dynamic_slice_in_dim(after_all, feature_start, local_width, 1)
    normed = lax.dynamic_slice_in_dim(normed_all, feature_start, local_width, 1)
    layer_out = plain_experts(normed, after, table, expert_weight, w_gate, w_up, w_down)
    return (layer_out, next_state_real, next_state_imaginary)


def solution(mesh):
    return jax.shard_map(
        body,
        mesh=mesh,
        in_specs=(
            P("ep", "tp"),
            P(),
            P(None, "tp"),
            P("tp", None),
            P("tp", None),
            P("tp"),
            P("tp", None, None),
            P("tp", None, None),
            P("tp", None, None),
            P("tp", None, None),
            P("tp"),
            P("ep", "tp", None),
            P("ep", "tp", None),
            P(),
            P(),
            P("ep", None),
            P("ep", None),
            P("ep", None, "tp"),
            P("ep", None, "tp"),
            P("ep", "tp", None),
        ),
        out_specs=(P("ep", "tp"), P("ep", "tp", None), P("ep", "tp", None)),
        check_vma=False,
    )
```

profile of v0, /device:TPU:0, one launch (start us, length us, event | category | flops | bytes accessed | tf_op | source)
XLA Modules:
  0.0 77.1 jit_solution(15477642599334810338)
XLA Ops:
  0.6 0.0 copy-start
  0.6 0.7 exp.6
  1.3 0.8 mul.152
  2.1 0.8 %add_divide_fusion = (f32[16,64]{1,0:T(8,128)S(1)}, f32[16,64]{1,0:T(8,128)S(1)}, f32[16,64]{1,0:T(8,128)S(1)}, f32[16,64]{1,0:T(8,128)S(1)}) fusion(f32[16,64]{1,0:T(8,128)} %param.24, f32[16,64]{1,0:T(8,128)} %param.23, f32[16]{0:T(128)S(1)} %exp.6), kind=kLoop, calls=%fused_computation.28 | loop fusion | flops 17408 | bytes 24640 | tf_op jit(solution)/shard_map/div | solution.py:33
  2.9 1.4 %copy.49.choice_ref = s32[64,2]{1,0:T(8,128)} copy(s32[64,2]{0,1:T(2,128)} %param.35) | data formatting | bytes 1024 | tf_op args[15]
  4.3 1.4 %copy.50.weight_ref = f32[64,2]{1,0:T(8,128)} copy(f32[64,2]{0,1:T(2,128)} %param.36) | data formatting | bytes 1024 | tf_op args[16]
  5.7 10.2 %shard_map.211 = (bf16[64,2048]{1,0:T(8,128)(2,1)}, bf16[64,256]{1,0:T(8,128)(2,1)}) custom-call(bf16[64,512]{1,0:T(8,128)(2,1)} %tokens_ref.1, f32[4,1,512]{2,1,0:T(1,128)} %bitcast.26, bf16[2048,256]{1,0:T(8,128)(2,1)} %weight_hbm.1), custom_call_target="tpu_custom_call" | custom-call | tf_op jit(solution)/shard_map/pallas_call | solution.py:407
  15.9 0.9 %copy.39 = bf16[64,256]{0,1:T(8,128)(2,1)S(1)} copy(bf16[64,256]{1,0:T(8,128)(2,1)} %get-tuple-element.5) | data formatting | bytes 65536 | tf_op jit(solution)/shard_map/pallas_call | solution.py:407
  16.7 1.3 %copy.37 = f32[64,16,64]{0,2,1:T(8,128)S(1)} copy(f32[64,16,64]{2,1,0:T(8,128)} %param.31) | data formatting | bytes 524288 | tf_op args[11]
  18.0 1.3 %copy.38 = f32[64,16,64]{0,2,1:T(8,128)S(1)} copy(f32[64,16,64]{2,1,0:T(8,128)} %param.32) | data formatting | bytes 524288 | tf_op args[12]
  19.3 1.8 %fusion = f32[64,16,64]{0,2,1:T(8,128)S(1)} fusion(bf16[64,16,16]{0,2,1:T(8,128)(2,1)S(1)} %bitcast.22, f32[64,16,64]{0,2,1:T(8,128)S(1)} %copy.37, f32[64,16,64]{0,2,1:T(8,128)S(1)} %copy.38, f32[16,64]{1,0:T(8,128)S(1)} %get-tuple-element.16, f32[16,64]{1,0:T(8,128)S(1)} %get-tuple-element.14, f32[16,64,16]{1,2,0:T(8,128)} %param.26, ...), kind=kOutput, calls=%fused_computation.1 | convolution fusion | flops 12894208 | bytes 966656 | tf_op jit(solution)/shard_map/sgc,gpc->sgp/dot_general | solution.py:41
  21.1 1.8 %fusion.1 = f32[64,16,64]{0,2,1:T(8,128)S(1)} fusion(bf16[64,16,16]{0,2,1:T(8,128)(2,1)S(1)} %bitcast.23, f32[64,16,64]{0,2,1:T(8,128)S(1)} %copy.38, f32[64,16,64]{0,2,1:T(8,128)S(1)} %copy.37, f32[16,64]{1,0:T(8,128)S(1)} %get-tuple-element.16, f32[16,64]{1,0:T(8,128)S(1)} %get-tuple-element.14, f32[16,64,16]{1,2,0:T(8,128)} %param.27, ...), kind=kOutput, calls=%fused_computation.3 | convolution fusion | flops 12894208 | bytes 966656 | tf_op jit(solution)/shard_map/sgc,gpc->sgp/dot_general | solution.py:40
  22.8 0.0 copy-done
  22.8 0.6 fusion.22
  23.4 1.5 %fusion.3 = f32[64,16,16]{0,2,1:T(8,128)S(1)} fusion(f32[16,64,16]{1,2,0:T(8,128)S(1)} %fusion.22, f32[64,16,64]{0,2,1:T(8,128)S(1)} %fusion, f32[16,16,64]{2,1,0:T(8,128)} %param.29, bf16[64,16,16]{0,2,1:T(8,128)(2,1)S(1)} %bitcast.24, f32[16,16]{1,0:T(8,128)S(1)} %mul.152), kind=kOutput, calls=%fused_computation.6 | convolution fusion | flops 12648448 | bytes 492544 | tf_op jit(solution)/shard_map/jdr,dyr->jdy/dot_general | solution.py:46
  24.9 1.0 %copy.52 = f32[64,16,64]{2,1,0:T(8,128)} copy(f32[64,16,64]{0,2,1:T(8,128)S(1)} %fusion) | data formatting | bytes 524288
  25.9 0.1 copy.48
  26.0 0.6 fusion.17.mixer_ref
  26.6 48.0 %shard_map.212 = bf16[64,512]{1,0:T(8,128)(2,1)} custom-call(bf16[64,256]{1,0:T(8,128)(2,1)} %fusion.17.mixer_ref, bf16[64,2048]{1,0:T(8,128)(2,1)} %get-tuple-element.6.tokens_ref, f32[1,2048]{1,0:T(1,128)} %bitcast.27, s32[64,2]{1,0:T(8,128)} %copy.49.choice_ref, f32[64,2]{1,0:T(8,128)} %copy.50.weight_ref, bf16[1024,2048]{1,0:T(8,128)(2,1)} %out_w_hbm.1, ...), custom_call_target="tpu_custom_call" | custom-call | tf_op jit(solution)/shard_map/pallas_call | solution.py:438
  74.6 1.0 %copy.51 = f32[64,16,64]{2,1,0:T(8,128)} copy(f32[64,16,64]{0,2,1:T(8,128)S(1)} %fusion.1) | data formatting | bytes 524288
  75.7 1.5 %copy.56 = bf16[64,512]{1,0:T(8,128)(2,1)} copy(bf16[64,512]{1,0:T(8,128)(2,1)} %shard_map.212) | data formatting | bytes 131072
Async XLA Ops:
  0.6 22.2 %copy-start = (f32[16,16,64]{2,1,0:T(8,128)S(1)}, f32[16,16,64]{2,1,0:T(8,128)}, u32[]{:S(2)}) copy-start(f32[16,16,64]{2,1,0:T(8,128)} %param.28) | copy-start | bytes 196612
where the time goes:
time: 77.7 us; the launch traced here: 77.1 us
  Pallas kernels  58.1 us (75%)
  local copies, waits for them, and re-layouts  11.3 us (15%)
  matrix products  5.55 us (7%)
  other arithmetic  1.48 us (2%)
    pallas_call x1, Pallas kernels, expert_call(): pl.pallas_call(functools.partial(expert_kernel, ep_count, tp_count), out_...  48 us
    pallas_call x1, Pallas kernels, gather_call(): pl.pallas_call(functools.partial(gather_kernel, tp_count), out_shape=(jax...  10.2 us
    unnamed x9, local copies, waits for them, and re-layouts  8.87 us
    dot_general x1, matrix products, state_step(): jnp.einsum('sgc,gpc->sgp', float_values, bbar_real, precision=highest_pre...  1.76 us
    dot_general x1, matrix products, state_step(): jnp.einsum('sgc,gpc->sgp', float_values, bbar_imag, precision=highest_pre...  1.76 us

commit v1 on v0

v1 whole, which is shorter than its diff:
```python
import functools
from types import SimpleNamespace

import jax
import jax.numpy as jnp
from jax import lax
from jax.experimental import pallas as pl
from jax.experimental.pallas import tpu as pltpu
from jax.sharding import PartitionSpec as P


def state_step(
    drive,
    real_state,
    imag_state,
    decay_rate,
    frequency,
    log_step,
    input_real,
    input_imag,
    readout_real,
    readout_imaginary,
    passthrough_scale,
):
    highest_precision = lax.Precision.HIGHEST
    count_of_groups, count_of_channels = (input_real.shape[0], input_real.shape[2])
    step = jnp.exp(log_step)[:, None]
    lam_real = -decay_rate
    magnitude = jnp.exp(lam_real * step)
    abar_real = magnitude * jnp.cos(frequency * step)
    abar_imag = magnitude * jnp.sin(frequency * step)
    denom = lam_real * lam_real + frequency * frequency
    numer = abar_real - 1.0
    factor_real = (numer * lam_real + abar_imag * frequency) / denom
    factor_imag = (abar_imag * lam_real - numer * frequency) / denom
    bbar_real = factor_real[..., None] * input_real - factor_imag[..., None] * input_imag
    bbar_imag = factor_real[..., None] * input_imag + factor_imag[..., None] * input_real
    float_values = drive.astype(jnp.float32).reshape(
        drive.shape[0], count_of_groups, count_of_channels
    )
    push_real = jnp.einsum("sgc,gpc->sgp", float_values, bbar_real, precision=highest_precision)
    push_imag = jnp.einsum("sgc,gpc->sgp", float_values, bbar_imag, precision=highest_precision)
    next_state_real = abar_real * real_state - abar_imag * imag_state + push_real
    next_state_imaginary = abar_real * imag_state + abar_imag * real_state + push_imag
    readout_matrix = (
        jnp.einsum("jdr,dyr->jdy", next_state_real, readout_real, precision=highest_precision)
        - jnp.einsum(
            "jdr,dyr->jdy", next_state_imaginary, readout_imaginary, precision=highest_precision
        )
        + passthrough_scale.reshape(count_of_groups, count_of_channels) * float_values
    )
    mixer = jax.nn.gelu(
        readout_matrix.reshape(drive.shape[0], count_of_groups * count_of_channels)
    ).astype(jnp.bfloat16)
    return (mixer, next_state_real, next_state_imaginary)


def slot_table(routes, expert_count, capacity):
    flat = routes.reshape(-1)
    onehot = (flat[:, None] == jnp.arange(expert_count, dtype=jnp.int32)[None, :]).astype(jnp.int32)
    before = jnp.cumsum(onehot, axis=0) - onehot
    slot = jnp.sum(before * onehot, axis=1)
    target = flat * capacity + slot
    return (
        target[None, :] == jnp.arange(expert_count * capacity, dtype=jnp.int32)[:, None]
    ).astype(jnp.bfloat16)


def flipped(index, mask, count):
    other = 0
    bit = 1
    while bit < count:
        digit = lax.rem(lax.div(index, bit), 2)
        other = other + bit * ((1 - digit) if mask & bit else digit)
        bit *= 2
    return other


def dot(left, right):
    return jnp.dot(left, right, preferred_element_type=jnp.float32)


def halves(values):
    high = values.astype(jnp.bfloat16)
    return high, (values - high.astype(jnp.float32)).astype(jnp.bfloat16)


def layer_kernel(ep_count, tp_count, sizes, *refs):
    names_in, names_out, names_scratch = sizes
    r = SimpleNamespace(**dict(zip(names_in + names_out + names_scratch, refs)))
    me_ep, me_tp = lax.axis_index("ep"), lax.axis_index("tp")
    capacity, width = r.out_tok.shape[1], r.out_tok.shape[2]
    channels = r.out_mix.shape[2]
    pairs = ep_count // 2
    slots = ep_count * capacity
    full = width * tp_count
    row_count = r.pieces.shape[1]
    f32, bf16 = jnp.float32, jnp.bfloat16
    tp_of = [flipped(me_tp, p, tp_count) for p in range(tp_count)]
    ep_of = [flipped(me_ep, j, ep_count) for j in range(ep_count)]

    barrier = pltpu.get_barrier_semaphore()
    for p in range(1, tp_count):
        pl.semaphore_signal(
            barrier, inc=1, device_id={"tp": tp_of[p]}, device_id_type=pl.DeviceIdType.MESH
        )
    for j in range(1, ep_count):
        pl.semaphore_signal(
            barrier, inc=1, device_id={"ep": ep_of[j]}, device_id_type=pl.DeviceIdType.MESH
        )

    loads = []

    def load(source, target):
        loads.append(pltpu.make_async_copy(source, target, r.load_sem.at[len(loads)]))
        loads[-1].start()
        return loads[-1]

    load_tokens = load(r.tokens, r.pieces.at[0])
    load_routes = [load(r.choice, r.choice_v), load(r.weight, r.weight_v)]
    load_small = [
        load(r.decay, r.decay_v),
        load(r.freq, r.freq_v),
        load(r.step, r.step_v),
        load(r.pass_, r.pass_v),
        load(r.gain_mix, r.gain_mix_v),
        load(r.gain_ffn, r.gain_ffn_v),
    ]
    load_mats = [
        load(r.in_re, r.in_re_v),
        load(r.in_im, r.in_im_v),
        load(r.re_re, r.re_re_v),
        load(r.re_im, r.re_im_v),
    ]
    load_w_in = load(r.w_in, r.w_in_v)
    load_states = [load(r.state_r, r.state_rv), load(r.state_i, r.state_iv)]
    load_w_out = load(r.w_out, r.w_out_v)
    load_gates = [load(r.gate.at[0], r.gate_v), load(r.up.at[0], r.up_v)]
    load_down = load(r.down.at[0], r.down_v)

    def remote(src, dst, send, recv, **where):
        return pltpu.make_async_remote_copy(
            src_ref=src,
            dst_ref=dst,
            send_sem=send,
            recv_sem=recv,
            device_id=where,
            device_id_type=pl.DeviceIdType.MESH,
        )

    started = []

    def go(copy):
        copy.start()
        started.append(copy)
        return copy

    load_tokens.wait()
    pl.semaphore_wait(barrier, tp_count - 1 + ep_count - 1)
    first = {
        p: go(remote(r.pieces.at[0], r.pieces.at[p], r.a_send.at[p], r.a_recv.at[p],
                     tp=tp_of[p]))
        for p in (3, 1, 2)
    }

    for copy in load_routes:
        copy.wait()
    choice, weight = r.choice_v[...], r.weight_v[...]
    top_count = choice.shape[0]
    experts = lax.broadcasted_iota(jnp.int32, (ep_count, row_count), 0)
    picks = [(choice[k : k + 1] == experts).astype(f32) for k in range(top_count)]
    earlier = (
        lax.broadcasted_iota(jnp.int32, (row_count, row_count), 0)
        < lax.broadcasted_iota(jnp.int32, (row_count, row_count), 1)
    ).astype(bf16)
    before = dot(sum(picks).astype(bf16), earlier)
    spots = lax.broadcasted_iota(jnp.int32, (slots, row_count), 0)
    table, weights = 0.0, 0.0
    for k in range(top_count):
        slot = jnp.sum(before * picks[k], axis=0, keepdims=True).astype(jnp.int32)
        hit = (choice[k : k + 1] * capacity + slot == spots).astype(f32)
        table = table + hit
        weights = weights + hit * weight[k : k + 1]
        before = before + picks[k]
    table = table.astype(bf16)
    r.table[...] = table.reshape(ep_count, capacity, row_count)
    r.out_tok[...] = dot(table, r.pieces[0]).astype(bf16).reshape(ep_count, capacity, width)

    def spread(source, arrived, send, recv):
        copies = {}
        for j in range(2, ep_count):
            copies[j] = go(remote(source.at[ep_of[j]], arrived.at[0, j], send.at[j], recv.at[j],
                                  ep=ep_of[j]))
        return copies

    tok_z = spread(r.out_tok, r.arr_tok, r.bz_send, r.bz_recv)
    tok_near, tok_far, mix_near, mix_far = {}, {}, {}, {}

    def forward(m, peers, z_copies, arrived, near, send, recv):
        for j in (2 * m, 2 * m + 1):
            z_copies[j].wait_recv()
        block = pl.ds(2 * m, 2)
        for p in peers:
            near[p, m] = go(remote(arrived.at[0, block], arrived.at[p, block], send.at[p, m],
                                   recv.at[p, m], tp=tp_of[p]))

    def tok_forward(m):
        forward(m, (1, 2), tok_z, r.arr_tok, tok_near, r.bn_send, r.bn_recv)

    def tok_relay(m):
        for p in (1, 2):
            tok_near[p, m].wait_recv()
            j = 2 * m + p - 1
            tok_far[p, m] = go(remote(r.arr_tok.at[p, j], r.arr_tok.at[3, j], r.bf_send.at[p, m],
                                      r.bf_recv.at[p, m], tp=tp_of[3 - p]))

    def share(pieces, shared, arrived, send, recv):
        for p in range(tp_count):
            piece = pieces[p]
            arrived[p, 0] = dot(r.table[me_ep], piece).astype(bf16)
            shared[p] = dot(r.table[ep_of[1]], piece).astype(bf16)
        return [
            go(remote(shared.at[p], arrived.at[p, 1], send.at[p], recv.at[p], ep=ep_of[1]))
            for p in range(tp_count)
        ]

    groups = r.decay.shape[0]
    entries = r.in_re_v.shape[1]
    per_group = channels // groups
    eye = (
        lax.broadcasted_iota(jnp.int32, (groups, groups), 0)
        == lax.broadcasted_iota(jnp.int32, (groups, groups), 1)
    ).astype(f32)
    for copy in load_small:
        copy.wait()
    step = jnp.sum(eye * jnp.exp(r.step_v[...]), axis=1, keepdims=True)
    lam = -r.decay_v[...]
    frequency = r.freq_v[...]
    magnitude = jnp.exp(lam * step)
    abar_real = magnitude * jnp.cos(frequency * step)
    abar_imag = magnitude * jnp.sin(frequency * step)
    denom = lam * lam + frequency * frequency
    numer = abar_real - 1.0
    factor_real = (numer * lam + abar_imag * frequency) / denom
    factor_imag = (abar_imag * lam - numer * frequency) / denom

    def per_channel(values):
        return jnp.broadcast_to(values[:, None, :], (groups, per_group, entries)).reshape(
            channels, entries
        )

    wide_real, wide_imag = per_channel(factor_real), per_channel(factor_imag)
    for copy in load_mats:
        copy.wait()
    in_re, in_im = r.in_re_v[...], r.in_im_v[...]
    push_w = jnp.concatenate(
        [wide_real * in_re - wide_imag * in_im, wide_real * in_im + wide_imag * in_re], axis=1
    )
    push_high, push_low = halves(push_w)
    r.push_w[0], r.push_w[1] = push_high, push_low
    read_w = jnp.concatenate([r.re_re_v[...], -r.re_im_v[...]], axis=1).T
    read_high, read_low = halves(read_w)
    r.read_w[0], r.read_w[1] = read_high, read_low
    weight_high, weight_low = halves(weights.T)
    r.combine[0], r.combine[1] = weight_high, weight_low
    rows = row_count * groups
    r.replicate[...] = (
        lax.broadcasted_iota(jnp.int32, (rows, row_count), 0) // groups
        == lax.broadcasted_iota(jnp.int32, (rows, row_count), 1)
    ).astype(bf16)
    r.own_group[...] = (
        lax.broadcasted_iota(jnp.int32, (groups, channels), 0)
        == lax.broadcasted_iota(jnp.int32, (groups, channels), 1) // per_group
    ).astype(f32)
    r.abar[0], r.abar[1] = abar_real, abar_imag

    early, middle, late = (range(1, pairs)[part] for part in (slice(1), slice(1, 2), slice(2, None)))
    for m in early:
        tok_forward(m)

    squares, drive = 0.0, None
    for p in (0, 1, 2, 3):
        if p:
            first[p].wait_recv()
        piece = r.pieces[p].astype(f32)
        squares = squares + jnp.sum(piece * piece, axis=1, keepdims=True)
        if not p:
            load_w_in.wait()
        term = dot((piece * r.gain_mix_v[tp_of[p]]).astype(bf16), r.w_in_v[tp_of[p]])
        drive = term if drive is None else drive + term
    drive = (drive * lax.rsqrt(squares / full + 1e-06)).astype(bf16)

    for m in middle:
        tok_forward(m)
    spread_drive = dot(r.replicate[...], drive).reshape(row_count, groups, channels)
    spread_drive = (spread_drive * r.own_group[...]).astype(bf16).reshape(rows, channels)
    push = dot(spread_drive, r.push_w[0]) + dot(spread_drive, r.push_w[1])
    for copy in load_states:
        copy.wait()

    def per_row(values):
        return jnp.broadcast_to(values[None], (row_count, groups, entries)).reshape(rows, entries)

    wide_real, wide_imag = per_row(r.abar[0]), per_row(r.abar[1])
    real, imag = r.state_rv[...], r.state_iv[...]
    next_real = wide_real * real - wide_imag * imag + push[:, :entries]
    next_imag = wide_real * imag + wide_imag * real + push[:, entries:]
    r.next_r[...] = next_real
    r.next_i[...] = next_imag
    for m in late:
        tok_forward(m)
    both_high, both_low = halves(jnp.concatenate([next_real, next_imag], axis=1))
    spread_y = (
        dot(both_high, r.read_w[0])
        + dot(both_low, r.read_w[0])
        + dot(both_high, r.read_w[1])
    )
    lane_group = lax.broadcasted_iota(jnp.int32, (row_count, 128), 1) // per_group
    lane_groups = 128 // per_group
    readout = []
    for t in range(channels // 128):
        r.spread_y[t] = spread_y[:, t * 128 : (t + 1) * 128]
        picked = None
        for g in range(lane_groups):
            strip = r.spread_y[t, pl.ds(t * lane_groups + g, row_count, groups), :]
            picked = strip if picked is None else jnp.where(lane_group == g, strip, picked)
        readout.append(picked)
    readout = jnp.concatenate(readout, axis=1) + r.pass_v[...] * drive.astype(f32)
    mixer = jax.nn.gelu(readout).astype(bf16)
    r.mixers[0] = mixer

    own_mix = {
        p: go(remote(r.mixers.at[0], r.mixers.at[p], r.e_send.at[p], r.e_recv.at[p], tp=tp_of[p]))
        for p in (3, 1, 2)
    }
    r.out_mix[...] = dot(table, mixer).astype(bf16).reshape(ep_count, capacity, channels)
    mix_z = spread(r.out_mix, r.arr_mix, r.cz_send, r.cz_recv)

    def mix_forward(m):
        forward(m, (3, 1, 2), mix_z, r.arr_mix, mix_near, r.cn_send, r.cn_recv)

    tok_share = share(r.pieces, r.shared_tok, r.arr_tok, r.bs_send, r.bs_recv)
    for m in range(1, pairs):
        tok_relay(m)
        mix_forward(m)
    for p in (1, 2, 3):
        own_mix[p].wait_recv()
    mix_share = share(r.mixers, r.shared_mix, r.arr_mix, r.cs_send, r.cs_recv)
    for copy in mix_share:
        copy.wait_recv()
    load_w_out.wait()
    mixed = r.mixed
    for p in (0, 1, 2):
        if p:
            for m in range(1, pairs):
                mix_near[p, m].wait_recv()
        block = r.arr_mix[p].reshape(slots, channels)
        for n in range(tp_count):
            columns = pl.ds(n * width, width)
            term = dot(block, r.w_out_v[tp_of[p], :, columns])
            mixed[:, columns] = term if p == 0 else mixed[:, columns] + term
    for copy in tok_share:
        copy.wait_recv()
    for m in range(1, pairs):
        mix_near[3, m].wait_recv()
        for p in (1, 2):
            tok_far[p, m].wait_recv()
    block = r.arr_mix[3].reshape(slots, channels)
    squares = 0.0
    for n in range(tp_count):
        columns = pl.ds(n * width, width)
        term = mixed[:, columns] + dot(block, r.w_out_v[tp_of[3], :, columns])
        after = r.arr_tok[tp_of[n]].reshape(slots, width).astype(f32)
        after = (after + term.astype(bf16).astype(f32)).astype(bf16).astype(f32)
        squares = squares + jnp.sum(after * after, axis=1, keepdims=True)
        r.normed[:, columns] = (after * r.gain_ffn_v[n]).astype(bf16)
    scale = lax.rsqrt(squares / full + 1e-06)

    r.scale[...] = jnp.broadcast_to(scale, r.scale.shape)
    for copy in load_gates:
        copy.wait()
    load_down.wait()
    hidden_width = r.hidden.shape[1]
    tile = next(t for t in (512, 256, 128) if hidden_width % t == 0)
    half = slots // 2

    def gate_up(first):
        span = pl.ds(first, half)

        @pl.loop(0, hidden_width // tile)
        def _(n):
            columns = pl.ds(pl.multiple_of(n * tile, tile), tile)
            scale = r.scale[span, :1]
            gate = dot(r.normed[span], r.gate_v[:, columns]) * scale
            upper = dot(r.normed[span], r.up_v[:, columns]) * scale
            r.hidden[span, columns] = (jax.nn.silu(gate) * upper).astype(bf16)

    def rows_of(j):
        return pl.ds(j * capacity, capacity)

    parts, relay_in, parts_in, held = r.parts, r.relay_in, r.parts_in, r.held
    far_send, pure_send, merged_send = {}, {}, {}

    def down(p, first):
        columns = pl.ds(pl.multiple_of(tp_of[p] * width, width), width)
        return dot(r.hidden[pl.ds(first, half)], r.down_v[:, columns])

    def down_far(first, chunk):
        parts[3, pl.ds(first, half)] = down(3, first).astype(bf16)
        for m in chunk:
            for p in (1, 2):
                j = 2 * m + p - 1
                far_send[p, m] = go(remote(parts.at[3, rows_of(j)], relay_in.at[rows_of(j)],
                                           r.rf_send.at[p, m], r.rf_recv.at[p, m], tp=tp_of[p]))

    def down_near(first, chunk):
        for p in (1, 2):
            value = down(p, first)
            held[p, pl.ds(first, half)] = value
            parts[p, pl.ds(first, half)] = value.astype(bf16)
            for m in chunk:
                j = 2 * m + p - 1
                pure_send[p, m] = go(remote(parts.at[p, rows_of(j)], parts_in.at[p, rows_of(j)],
                                            r.rp_send.at[p, m], r.rp_recv.at[p, m], tp=tp_of[p]))

    def down_own(first):
        held[0, pl.ds(first, half)] = down(0, first)

    def merge(m):
        for p in (1, 2):
            q = 3 - p
            j = 2 * m + p - 1
            far_send[p, m].wait_recv()
            merged = held[q, rows_of(j)] + relay_in[rows_of(j)].astype(f32)
            r.merged[rows_of(j)] = merged.astype(bf16)
            merged_send[q, m] = go(remote(r.merged.at[rows_of(j)], parts_in.at[q, rows_of(j)],
                                          r.rm_send.at[q, m], r.rm_recv.at[q, m], tp=tp_of[q]))

    back = {}

    def finish(m):
        for p in (1, 2):
            pure_send[p, m].wait_recv()
            merged_send[p, m].wait_recv()
        span = pl.ds(2 * m * capacity, 2 * capacity)
        total = held[0, span] + parts_in[1, span].astype(f32) + parts_in[2, span].astype(f32)
        r.results[pl.ds(2 * m, 2)] = total.astype(bf16).reshape(2, capacity, width)
        for j in (2 * m + 1, 2 * m):
            if j:
                back[j] = go(remote(r.results.at[j], r.returned.at[me_ep],
                                    r.z_send.at[j], r.z_recv.at[j], ep=ep_of[j]))

    far_half = tuple(reversed(range(pairs // 2, pairs)))
    near_half = tuple(reversed(range(pairs // 2)))
    gate_up(half)
    down_far(half, far_half)
    down_near(half, far_half)
    down_own(half)
    gate_up(0)
    for m in far_half:
        merge(m)
    down_far(0, near_half)
    down_near(0, near_half)
    down_own(0)
    for m in far_half:
        finish(m)
    for m in near_half:
        merge(m)
    for m in near_half[:-1]:
        finish(m)
    own = pl.ds(pl.multiple_of(me_tp * width, width), width)
    mixed_own = None
    for p in range(tp_count):
        term = dot(r.mixers[p], r.w_out_v[tp_of[p], :, own])
        mixed_own = term if mixed_own is None else mixed_own + term
    after_own = (
        (r.pieces[0].astype(f32) + mixed_own.astype(bf16).astype(f32)).astype(bf16).astype(f32)
    )
    finish(0)
    r.returned[me_ep] = r.results[0]
    for j in range(1, ep_count):
        remote(r.results.at[j], r.returned.at[ep_of[j]], r.z_send.at[j],
               r.z_recv.at[j], ep=ep_of[j]).wait_recv()
    everything = r.returned[...].reshape(slots, width)
    weighted = dot(r.combine[0], everything) + dot(r.combine[1], everything)
    r.out[...] = (after_own + weighted).astype(bf16)
    for copy in started:
        copy.wait_send()


def layer_call(
    tokens, gain_mix, w_in, decay_rate, frequency, log_step, input_real, input_imag, readout_real,
    readout_imaginary, passthrough_scale, state_real, state_imag, w_out, gain_ffn, expert_choice,
    expert_weight, w_gate, w_up, w_down, capacity, ep_count, tp_count,
):
    row_count, width = tokens.shape
    full = width * tp_count
    groups, entries, per_group = input_real.shape
    channels = groups * per_group
    slots = ep_count * capacity
    pairs = ep_count // 2
    hidden_width = w_gate.shape[2]
    rows = row_count * groups
    bf16, f32 = jnp.bfloat16, jnp.float32
    vmem = pl.BlockSpec(memory_space=pltpu.VMEM)
    hbm = pl.BlockSpec(memory_space=pl.ANY)
    inputs = dict(
        tokens=(tokens, hbm),
        gain_mix=(gain_mix.reshape(tp_count, 1, width), hbm),
        gain_ffn=(gain_ffn.reshape(tp_count, 1, width), hbm),
        decay=(decay_rate, hbm),
        freq=(frequency, hbm),
        step=(log_step.reshape(1, groups), hbm),
        pass_=(passthrough_scale.reshape(1, channels), hbm),
        choice=(expert_choice.T, hbm),
        weight=(expert_weight.T, hbm),
        in_re=(jnp.transpose(input_real, (0, 2, 1)).reshape(channels, entries), hbm),
        in_im=(jnp.transpose(input_imag, (0, 2, 1)).reshape(channels, entries), hbm),
        re_re=(readout_real.reshape(channels, entries), hbm),
        re_im=(readout_imaginary.reshape(channels, entries), hbm),
        state_r=(state_real.reshape(rows, entries), hbm),
        state_i=(state_imag.reshape(rows, entries), hbm),
        w_in=(w_in.reshape(tp_count, width, channels), hbm),
        w_out=(w_out.reshape(tp_count, channels, full), hbm),
        gate=(w_gate, hbm),
        up=(w_up, hbm),
        down=(w_down, hbm),
    )
    outputs = dict(
        out=pltpu.VMEM((row_count, width), bf16),
        next_r=pltpu.VMEM((rows, entries), f32),
        next_i=pltpu.VMEM((rows, entries), f32),
    )
    dma = lambda *shape: pltpu.SemaphoreType.DMA(shape)
    scratch = dict(
        pieces=pltpu.VMEM((tp_count, row_count, width), bf16),
        choice_v=pltpu.VMEM(expert_choice.shape[::-1], expert_choice.dtype),
        weight_v=pltpu.VMEM(expert_weight.shape[::-1], f32),
        decay_v=pltpu.VMEM((groups, entries), f32),
        freq_v=pltpu.VMEM((groups, entries), f32),
        step_v=pltpu.VMEM((1, groups), f32),
        pass_v=pltpu.VMEM((1, channels), f32),
        gain_mix_v=pltpu.VMEM((tp_count, 1, width), f32),
        gain_ffn_v=pltpu.VMEM((tp_count, 1, width), f32),
        table=pltpu.VMEM((ep_count, capacity, row_count), bf16),
        replicate=pltpu.VMEM((rows, row_count), bf16),
        own_group=pltpu.VMEM((groups, channels), f32),
        abar=pltpu.VMEM((2, groups, entries), f32),
        shared_tok=pltpu.VMEM((tp_count, capacity, width), bf16),
        shared_mix=pltpu.VMEM((tp_count, capacity, channels), bf16),
        scale=pltpu.VMEM((slots, 128), f32),
        in_re_v=pltpu.VMEM((channels, entries), f32),
        in_im_v=pltpu.VMEM((channels, entries), f32),
        re_re_v=pltpu.VMEM((channels, entries), f32),
        re_im_v=pltpu.VMEM((channels, entries), f32),
        state_rv=pltpu.VMEM((rows, entries), f32),
        state_iv=pltpu.VMEM((rows, entries), f32),
        w_in_v=pltpu.VMEM((tp_count, width, channels), bf16),
        w_out_v=pltpu.VMEM((tp_count, channels, full), bf16),
        gate_v=pltpu.VMEM((full, hidden_width), bf16),
        up_v=pltpu.VMEM((full, hidden_width), bf16),
        down_v=pltpu.VMEM((hidden_width, full), bf16),
        push_w=pltpu.VMEM((2, channels, 2 * entries), bf16),
        read_w=pltpu.VMEM((2, 2 * entries, channels), bf16),
        combine=pltpu.VMEM((2, row_count, slots), bf16),
        spread_y=pltpu.VMEM((channels // 128, rows, 128), f32),
        mixers=pltpu.VMEM((tp_count, row_count, channels), bf16),
        out_tok=pltpu.VMEM((ep_count, capacity, width), bf16),
        arr_tok=pltpu.VMEM((tp_count, ep_count, capacity, width), bf16),
        out_mix=pltpu.VMEM((ep_count, capacity, channels), bf16),
        arr_mix=pltpu.VMEM((tp_count, ep_count, capacity, channels), bf16),
        mixed=pltpu.VMEM((slots, full), f32),
        normed=pltpu.VMEM((slots, full), bf16),
        hidden=pltpu.VMEM((slots, hidden_width), bf16),
        parts=pltpu.VMEM((tp_count, slots, width), bf16),
        held=pltpu.VMEM((3, slots, width), f32),
        relay_in=pltpu.VMEM((slots, width), bf16),
        merged=pltpu.VMEM((slots, width), bf16),
        parts_in=pltpu.VMEM((3, slots, width), bf16),
        results=pltpu.VMEM((ep_count, capacity, width), bf16),
        returned=pltpu.VMEM((ep_count, capacity, width), bf16),
        load_sem=dma(20),
    )
    kinds = dict(
        a=(tp_count,), e=(tp_count,), bs=(tp_count,), cs=(tp_count,), bz=(ep_count,), cz=(ep_count,), z=(ep_count,),
        bn=(3, pairs), bf=(3, pairs), cn=(4, pairs),
        rf=(3, pairs), rp=(3, pairs), rm=(3, pairs),
    )
    for name, shape in kinds.items():
        scratch[name + "_send"], scratch[name + "_recv"] = dma(*shape), dma(*shape)
    names = (tuple(inputs), tuple(outputs), tuple(scratch))
    out, next_real, next_imag = pl.pallas_call(
        functools.partial(layer_kernel, ep_count, tp_count, names),
        out_shape=tuple(outputs.values()),
        in_specs=[spec for _, spec in inputs.values()],
        out_specs=(vmem, vmem, vmem),
        scratch_shapes=list(scratch.values()),
        compiler_params=pltpu.CompilerParams(
            collective_id=0, has_side_effects=True, vmem_limit_bytes=60 * 1024 * 1024
        ),
    )(*[value for value, _ in inputs.values()])
    shape = (row_count, groups, entries)
    return out, next_real.reshape(shape), next_imag.reshape(shape)


def plain_experts(normed, after, table, expert_weight, w_gate, w_up, w_down):
    row_count, top_count = expert_weight.shape
    expert_count = lax.axis_size("ep")
    capacity = table.shape[0] // expert_count
    width = normed.shape[1]
    repeated = jnp.repeat(normed, top_count, axis=0)
    sent = jnp.dot(table, repeated, preferred_element_type=jnp.float32).astype(jnp.bfloat16)
    sent = sent.reshape(expert_count, capacity, width)
    arrived = lax.all_to_all(sent, "ep", split_axis=0, concat_axis=0, tiled=True)
    flat = arrived.reshape(expert_count * capacity, width)
    piece = lax.all_gather(flat, "tp", axis=1, tiled=True)
    gate = jnp.dot(piece, w_gate[0], preferred_element_type=jnp.float32)
    upper = jnp.dot(piece, w_up[0], preferred_element_type=jnp.float32)
    hidden = (jax.nn.silu(gate) * upper).astype(jnp.bfloat16)
    partial_value = jnp.dot(hidden, w_down[0], preferred_element_type=jnp.float32)
    summed = lax.psum_scatter(
        partial_value.astype(jnp.bfloat16), "tp", scatter_dimension=1, tiled=True
    )
    results = summed.reshape(expert_count, capacity, width)
    returned = lax.all_to_all(results, "ep", split_axis=0, concat_axis=0, tiled=True)
    returned = returned.reshape(expert_count * capacity, width)
    picked = jnp.dot(table.T, returned, preferred_element_type=jnp.float32)
    picked = picked.reshape(row_count, top_count, width)
    weighted = jnp.sum(picked * expert_weight[..., None], axis=1)
    return (after.astype(jnp.float32) + weighted).astype(jnp.bfloat16)


def norm(values, gains):
    floats = values.astype(jnp.float32)
    scale = lax.rsqrt(jnp.mean(floats * floats, axis=1, keepdims=True) + 1e-06)
    return (floats * scale * gains).astype(jnp.bfloat16)


def power_of_two(count):
    return count & (count - 1) == 0


def body(
    tokens,
    gain_mix,
    w_in,
    decay_rate,
    frequency,
    log_step,
    input_real,
    input_imag,
    readout_real,
    readout_imaginary,
    passthrough_scale,
    state_real,
    state_imag,
    w_out,
    gain_ffn,
    expert_choice,
    expert_weight,
    w_gate,
    w_up,
    w_down,
):
    tp_count = lax.axis_size("tp")
    expert_count = lax.axis_size("ep")
    row_count, local_width = tokens.shape
    feature_start = lax.axis_index("tp") * local_width
    top_count = expert_choice.shape[1]
    capacity = 2 * row_count * top_count // expert_count
    fused = (
        local_width % 128 == 0
        and w_gate.shape[2] % 128 == 0
        and capacity % 16 == 0
        and tp_count == 4
        and power_of_two(expert_count)
        and 4 <= expert_count <= 8
        and w_in.shape[1] % 128 == 0
        and row_count % 16 == 0
        and input_real.shape[0] % 8 == 0
        and input_real.shape[1] == 64
        and 128 % input_real.shape[2] == 0
    )
    if fused:
        return layer_call(
            tokens,
            gain_mix,
            w_in,
            decay_rate,
            frequency,
            log_step,
            input_real,
            input_imag,
            readout_real,
            readout_imaginary,
            passthrough_scale,
            state_real,
            state_imag,
            w_out,
            gain_ffn,
            expert_choice,
            expert_weight,
            w_gate,
            w_up,
            w_down,
            capacity,
            expert_count,
            tp_count,
        )
    all_tokens = lax.all_gather(tokens, "tp", axis=1, tiled=True)
    drive = jnp.dot(
        norm(all_tokens, gain_mix), w_in, preferred_element_type=jnp.float32
    ).astype(jnp.bfloat16)
    mixer, next_state_real, next_state_imaginary = state_step(
        drive,
        state_real,
        state_imag,
        decay_rate,
        frequency,
        log_step,
        input_real,
        input_imag,
        readout_real,
        readout_imaginary,
        passthrough_scale,
    )
    table = slot_table(expert_choice, expert_count, capacity)
    mixed = jnp.dot(
        lax.all_gather(mixer, "tp", axis=1, tiled=True), w_out, preferred_element_type=jnp.float32
    ).astype(jnp.bfloat16)
    after_all = (all_tokens.astype(jnp.float32) + mixed.astype(jnp.float32)).astype(jnp.bfloat16)
    normed_all = norm(after_all, gain_ffn)
    after = lax.dynamic_slice_in_dim(after_all, feature_start, local_width, 1)
    normed = lax.dynamic_slice_in_dim(normed_all, feature_start, local_width, 1)
    layer_out = plain_experts(normed, after, table, expert_weight, w_gate, w_up, w_down)
    return (layer_out, next_state_real, next_state_imaginary)


def solution(mesh):
    return jax.shard_map(
        body,
        mesh=mesh,
        in_specs=(
            P("ep", "tp"),
            P(),
            P(None, "tp"),
            P("tp", None),
            P("tp", None),
            P("tp"),
            P("tp", None, None),
            P("tp", None, None),
            P("tp", None, None),
            P("tp", None, None),
            P("tp"),
            P("ep", "tp", None),
            P("ep", "tp", None),
            P(),
            P(),
            P("ep", None),
            P("ep", None),
            P("ep", None, "tp"),
            P("ep", None, "tp"),
            P("ep", "tp", None),
        ),
        out_specs=(P("ep", "tp"), P("ep", "tp", None), P("ep", "tp", None)),
        check_vma=False,
    )
```

time: 77.7 us -> 51 us (0.66)
  Pallas kernels: 58.1 us -> 48 us
  local copies, waits for them, and re-layouts: 11.3 us -> 2.22 us
  matrix products: 5.55 us -> 0 us
  other arithmetic: 1.48 us -> 0 us
    pallas_call x2 -> x1, Pallas kernels: 58.1 us -> 48 us  [layer_call(): pl.pallas_call(functools.partial(layer_kernel, ep_count, tp_count, names)...]
    unnamed x9 -> x3, local copies, waits for them, and re-layouts: 8.87 us -> 2.22 us
    dot_general x4 -> x0, matrix products: 5.55 us -> none  [the longest x1 1.76 us: state_step(): jnp.einsum('sgc,gpc->sgp', float_values, bbar_real, precision=highest_pre...]
    pallas_call x1 -> x0, local copies, waits for them, and re-layouts: 0.87 us -> none  [gather_call(): pl.pallas_call(functools.partial(gather_kernel, tp_count), out_shape=(jax...]
    div x1 -> x0, other arithmetic: 0.84 us -> none  [state_step(): factor_real = (numer * lam_real + abar_imag * frequency) / denom]
where the time goes in v1:
time: 51 us; the launch traced here: 50.8 us
  Pallas kernels  48 us (94%)
  local copies, waits for them, and re-layouts  2.22 us (4%)
  between operations  0.65 us (1%)
    pallas_call x1, Pallas kernels, layer_call(): pl.pallas_call(functools.partial(layer_kernel, ep_count, tp_count, names)...  48 us
    unnamed x3, local copies, waits for them, and re-layouts  2.22 us

profile of v1, /device:TPU:0, one launch (start us, length us, event | category | flops | bytes accessed | tf_op | source)
XLA Modules:
  0.0 50.8 jit_solution(15074247576715122984)
XLA Ops:
  0.6 48.0 %shard_map.211 = (bf16[64,512]{1,0:T(8,128)(2,1)S(1)}, f32[1024,64]{1,0:T(8,128)S(1)}, f32[1024,64]{1,0:T(8,128)S(1)}) custom-call(bf16[64,512]{1,0:T(8,128)(2,1)} %refs_0_.1, f32[4,1,512]{2,1,0:T(1,128)} %bitcast.30, f32[4,1,512]{2,1,0:T(1,128)} %bitcast.31, f32[16,64]{1,0:T(8,128)} %refs_3_.1, f32[16,64]{1,0:T(8,128)} %refs_4_.1, f32[1,16]{1,0:T(1,128)} %bitcast.35, ...), custom_call_target="tpu_custom_call" | custom-call | tf_op jit(solution)/shard_map/pallas_call | solution.py:592
  48.6 0.6 %copy.26 = bf16[64,512]{1,0:T(8,128)(2,1)} copy(bf16[64,512]{1,0:T(8,128)(2,1)S(1)} %get-tuple-element.9) | data formatting | bytes 131072
  49.3 0.8 %copy.27 = f32[64,16,64]{2,1,0:T(8,128)} copy(f32[64,16,64]{2,1,0:T(8,128)S(1)} %bitcast.21) | data formatting | bytes 524288
  50.1 0.8 %copy.28 = f32[64,16,64]{2,1,0:T(8,128)} copy(f32[64,16,64]{2,1,0:T(8,128)S(1)} %bitcast.20) | data formatting | bytes 524288

commit v2 on v1

--- a/solution.py
+++ b/solution.py
@@ -186,14 +186,14 @@
     r.table[...] = table.reshape(ep_count, capacity, row_count)
     r.out_tok[...] = dot(table, r.pieces[0]).astype(bf16).reshape(ep_count, capacity, width)
 
-    def spread(source, arrived, send, recv):
+    def spread(order, source, arrived, send, recv):
         copies = {}
-        for j in range(2, ep_count):
+        for j in order:
             copies[j] = go(remote(source.at[ep_of[j]], arrived.at[0, j], send.at[j], recv.at[j],
                                   ep=ep_of[j]))
         return copies
 
-    tok_z = spread(r.out_tok, r.arr_tok, r.bz_send, r.bz_recv)
+    tok_z = spread(range(2, ep_count), r.out_tok, r.arr_tok, r.bz_send, r.bz_recv)
     tok_near, tok_far, mix_near, mix_far = {}, {}, {}, {}
 
     def forward(m, peers, z_copies, arrived, near, send, recv):
@@ -257,10 +257,10 @@
         [wide_real * in_re - wide_imag * in_im, wide_real * in_im + wide_imag * in_re], axis=1
     )
     push_high, push_low = halves(push_w)
-    r.push_w[0], r.push_w[1] = push_high, push_low
+    r.push_w[...] = jnp.concatenate([push_high, push_low], axis=1)
     read_w = jnp.concatenate([r.re_re_v[...], -r.re_im_v[...]], axis=1).T
     read_high, read_low = halves(read_w)
-    r.read_w[0], r.read_w[1] = read_high, read_low
+    r.read_w[...] = jnp.concatenate([read_high, read_low], axis=0)
     weight_high, weight_low = halves(weights.T)
     r.combine[0], r.combine[1] = weight_high, weight_low
     rows = row_count * groups
@@ -274,12 +274,12 @@
     ).astype(f32)
     r.abar[0], r.abar[1] = abar_real, abar_imag
 
+    squares, drive = 0.0, None
     early, middle, late = (range(1, pairs)[part] for part in (slice(1), slice(1, 2), slice(2, None)))
-    for m in early:
-        tok_forward(m)
-
-    squares, drive = 0.0, None
     for p in (0, 1, 2, 3):
+        if p == 3:
+            for m in early:
+                tok_forward(m)
         if p:
             first[p].wait_recv()
         piece = r.pieces[p].astype(f32)
@@ -294,7 +294,8 @@
         tok_forward(m)
     spread_drive = dot(r.replicate[...], drive).reshape(row_count, groups, channels)
     spread_drive = (spread_drive * r.own_group[...]).astype(bf16).reshape(rows, channels)
-    push = dot(spread_drive, r.push_w[0]) + dot(spread_drive, r.push_w[1])
+    push = dot(spread_drive, r.push_w[...])
+    push = push[:, : 2 * entries] + push[:, 2 * entries :]
     for copy in load_states:
         copy.wait()
 
@@ -307,14 +308,8 @@
     next_imag = wide_real * imag + wide_imag * real + push[:, entries:]
     r.next_r[...] = next_real
     r.next_i[...] = next_imag
-    for m in late:
-        tok_forward(m)
-    both_high, both_low = halves(jnp.concatenate([next_real, next_imag], axis=1))
-    spread_y = (
-        dot(both_high, r.read_w[0])
-        + dot(both_low, r.read_w[0])
-        + dot(both_high, r.read_w[1])
-    )
+    both = jnp.concatenate([next_real, next_imag], axis=1).astype(bf16)
+    spread_y = dot(jnp.concatenate([both, both], axis=1), r.read_w[...])
     lane_group = lax.broadcasted_iota(jnp.int32, (row_count, 128), 1) // per_group
     lane_groups = 128 // per_group
     readout = []
@@ -329,67 +324,91 @@
     mixer = jax.nn.gelu(readout).astype(bf16)
     r.mixers[0] = mixer
 
-    own_mix = {
-        p: go(remote(r.mixers.at[0], r.mixers.at[p], r.e_send.at[p], r.e_recv.at[p], tp=tp_of[p]))
-        for p in (3, 1, 2)
-    }
     r.out_mix[...] = dot(table, mixer).astype(bf16).reshape(ep_count, capacity, channels)
-    mix_z = spread(r.out_mix, r.arr_mix, r.cz_send, r.cz_recv)
+    far_first = [j for m in reversed(range(1, pairs)) for j in (2 * m, 2 * m + 1)]
+    mix_z = spread(far_first, r.out_mix, r.arr_mix, r.cz_send, r.cz_recv)
+    far_half = tuple(reversed(range(pairs // 2, pairs)))
+    near_half = tuple(reversed(range(pairs // 2)))
+    half = slots // 2
+    blocks = ep_count // 2
 
     def mix_forward(m):
-        forward(m, (3, 1, 2), mix_z, r.arr_mix, mix_near, r.cn_send, r.cn_recv)
-
+        forward(m, (1, 2, 3), mix_z, r.arr_mix, mix_near, r.cn_send, r.cn_recv)
+
+    for m in late:
+        tok_forward(m)
+    for m in reversed(far_half[1:]):
+        tok_relay(m)
+    mix_forward(far_half[0])
+    tok_relay(far_half[0])
+    for m in far_half[1:]:
+        mix_forward(m)
     tok_share = share(r.pieces, r.shared_tok, r.arr_tok, r.bs_send, r.bs_recv)
-    for m in range(1, pairs):
-        tok_relay(m)
-        mix_forward(m)
-    for p in (1, 2, 3):
-        own_mix[p].wait_recv()
-    mix_share = share(r.mixers, r.shared_mix, r.arr_mix, r.cs_send, r.cs_recv)
-    for copy in mix_share:
-        copy.wait_recv()
-    load_w_out.wait()
+
+    def near_traffic():
+        copies = {
+            p: go(remote(r.mixers.at[0], r.mixers.at[p], r.e_send.at[p], r.e_recv.at[p],
+                         tp=tp_of[p]))
+            for p in (3, 1, 2)
+        }
+        for m in near_half[:-1]:
+            tok_relay(m)
+            mix_forward(m)
+        return copies
+
     mixed = r.mixed
-    for p in (0, 1, 2):
-        if p:
-            for m in range(1, pairs):
-                mix_near[p, m].wait_recv()
-        block = r.arr_mix[p].reshape(slots, channels)
+
+    def mix_rows(chunk, then=None):
+        block = pl.ds(2 * chunk[-1], blocks)
+        span = pl.ds(2 * chunk[-1] * capacity, half)
+        remote_chunk = [m for m in chunk if m]
+        early = range(tp_count - 1) if chunk is far_half else ()
+        for p in early:
+            if p:
+                for m in remote_chunk:
+                    mix_near[p, m].wait_recv()
+            rows_of_p = r.arr_mix[p, block].reshape(half, channels)
+            for n in range(tp_count):
+                columns = pl.ds(n * width, width)
+                term = dot(rows_of_p, r.w_out_v[tp_of[p], :, columns])
+                mixed[span, columns] = term if p == 0 else mixed[span, columns] + term
+        result = then() if then else None
+        for m in remote_chunk:
+            for p in (1, 2, 3):
+                if p == 3 or not early:
+                    mix_near[p, m].wait_recv()
+            for p in (1, 2):
+                tok_far[p, m].wait_recv()
+        rest = [p for p in range(tp_count) if p not in early]
+        squares = 0.0
         for n in range(tp_count):
             columns = pl.ds(n * width, width)
-            term = dot(block, r.w_out_v[tp_of[p], :, columns])
-            mixed[:, columns] = term if p == 0 else mixed[:, columns] + term
-    for copy in tok_share:
-        copy.wait_recv()
-    for m in range(1, pairs):
-        mix_near[3, m].wait_recv()
-        for p in (1, 2):
-            tok_far[p, m].wait_recv()
-    block = r.arr_mix[3].reshape(slots, channels)
-    squares = 0.0
-    for n in range(tp_count):
-        columns = pl.ds(n * width, width)
-        term = mixed[:, columns] + dot(block, r.w_out_v[tp_of[3], :, columns])
-        after = r.arr_tok[tp_of[n]].reshape(slots, width).astype(f32)
-        after = (after + term.astype(bf16).astype(f32)).astype(bf16).astype(f32)
-        squares = squares + jnp.sum(after * after, axis=1, keepdims=True)
-        r.normed[:, columns] = (after * r.gain_ffn_v[n]).astype(bf16)
-    scale = lax.rsqrt(squares / full + 1e-06)
-
-    r.scale[...] = jnp.broadcast_to(scale, r.scale.shape)
+            term = mixed[span, columns] if early else 0.0
+            for p in rest:
+                rows_of_p = r.arr_mix[p, block].reshape(half, channels)
+                term = term + dot(rows_of_p, r.w_out_v[tp_of[p], :, columns])
+            after = r.arr_tok[tp_of[n], block].reshape(half, width).astype(f32)
+            after = (after + term.astype(bf16).astype(f32)).astype(bf16).astype(f32)
+            squares = squares + jnp.sum(after * after, axis=1, keepdims=True)
+            r.normed[span, columns] = (after * r.gain_ffn_v[n]).astype(bf16)
+        scale = lax.rsqrt(squares / full + 1e-06)
+        r.scale[span] = jnp.broadcast_to(scale, (half, 128))
+        return result
+
+    load_w_out.wait()
+    own_mix = mix_rows(far_half, near_traffic)
     for copy in load_gates:
         copy.wait()
     load_down.wait()
     hidden_width = r.hidden.shape[1]
     tile = next(t for t in (512, 256, 128) if hidden_width % t == 0)
-    half = slots // 2
-
-    def gate_up(first):
+    tiles = hidden_width // tile
+
+    def gate_up(first, start, stop):
         span = pl.ds(first, half)
 
-        @pl.loop(0, hidden_width // tile)
-        def _(n):
-            columns = pl.ds(pl.multiple_of(n * tile, tile), tile)
+        for n in range(start, stop):
+            columns = pl.ds(n * tile, tile)
             scale = r.scale[span, :1]
             gate = dot(r.normed[span], r.gate_v[:, columns]) * scale
             upper = dot(r.normed[span], r.up_v[:, columns]) * scale
@@ -450,20 +469,25 @@
                 back[j] = go(remote(r.results.at[j], r.returned.at[me_ep],
                                     r.z_send.at[j], r.z_recv.at[j], ep=ep_of[j]))
 
-    far_half = tuple(reversed(range(pairs // 2, pairs)))
-    near_half = tuple(reversed(range(pairs // 2)))
-    gate_up(half)
+    gate_up(half, 0, tiles)
+    for p in (1, 2, 3):
+        own_mix[p].wait_recv()
+    mix_share = share(r.mixers, r.shared_mix, r.arr_mix, r.cs_send, r.cs_recv)
     down_far(half, far_half)
     down_near(half, far_half)
     down_own(half)
-    gate_up(0)
+    for copy in tok_share + mix_share:
+        copy.wait_recv()
+    mix_rows(near_half)
+    gate_up(0, 0, tiles // 2)
     for m in far_half:
         merge(m)
+    gate_up(0, tiles // 2, tiles)
     down_far(0, near_half)
     down_near(0, near_half)
-    down_own(0)
     for m in far_half:
         finish(m)
+    down_own(0)
     for m in near_half:
         merge(m)
     for m in near_half[:-1]:
@@ -486,6 +510,14 @@
     r.out[...] = (after_own + weighted).astype(bf16)
     for copy in started:
         copy.wait_send()
+
+
+def write_kernel(*refs):
+    copies = [pltpu.make_async_copy(refs[k], refs[3 + k], refs[6].at[k]) for k in range(3)]
+    for copy in copies:
+        copy.start()
+    for copy in copies:
+        copy.wait()
 
 
 def layer_call(
@@ -560,8 +592,8 @@
         gate_v=pltpu.VMEM((full, hidden_width), bf16),
         up_v=pltpu.VMEM((full, hidden_width), bf16),
         down_v=pltpu.VMEM((hidden_width, full), bf16),
-        push_w=pltpu.VMEM((2, channels, 2 * entries), bf16),
-        read_w=pltpu.VMEM((2, 2 * entries, channels), bf16),
+        push_w=pltpu.VMEM((channels, 4 * entries), bf16),
+        read_w=pltpu.VMEM((4 * entries, channels), bf16),
         combine=pltpu.VMEM((2, row_count, slots), bf16),
         spread_y=pltpu.VMEM((channels // 128, rows, 128), f32),
         mixers=pltpu.VMEM((tp_count, row_count, channels), bf16),
@@ -599,6 +631,14 @@
             collective_id=0, has_side_effects=True, vmem_limit_bytes=60 * 1024 * 1024
         ),
     )(*[value for value, _ in inputs.values()])
+    results = [pltpu.with_memory_space_constraint(x, pltpu.VMEM) for x in (out, next_real, next_imag)]
+    out, next_real, next_imag = pl.pallas_call(
+        write_kernel,
+        out_shape=tuple(jax.ShapeDtypeStruct(x.shape, x.dtype) for x in results),
+        in_specs=[vmem] * 3,
+        out_specs=(hbm, hbm, hbm),
+        scratch_shapes=[dma(3)],
+    )(*results)
     shape = (row_count, groups, entries)
     return out, next_real.reshape(shape), next_imag.reshape(shape)
 

time: 51 us -> 45.4 us (0.89)
  Pallas kernels: 48 us -> 44.6 us
  local copies, waits for them, and re-layouts: 2.22 us -> 0 us
    pallas_call x1, Pallas kernels: 48 us -> 43.6 us  [layer_call(): pl.pallas_call(functools.partial(layer_kernel, ep_count, tp_count, names)...]
    unnamed x3 -> x0, local copies, waits for them, and re-layouts: 2.22 us -> none
    pallas_call x0 -> x1, Pallas kernels: none -> 1.02 us  [layer_call(): pl.pallas_call(write_kernel, out_shape=tuple((jax.ShapeDtypeStruct(x.shap...]
where the time goes in v2:
time: 45.4 us; the launch traced here: 45.3 us
  Pallas kernels  44.6 us (98%)
  between operations  0.65 us (1%)
    pallas_call x1, Pallas kernels, layer_call(): pl.pallas_call(functools.partial(layer_kernel, ep_count, tp_count, names)...  43.6 us
    pallas_call x1, Pallas kernels, layer_call(): pl.pallas_call(write_kernel, out_shape=tuple((jax.ShapeDtypeStruct(x.shap...  1.02 us

profile of v2, /device:TPU:0, one launch (start us, length us, event | category | flops | bytes accessed | tf_op | source)
XLA Modules:
  0.0 45.3 jit_solution(1682057930989222542)
XLA Ops:
  0.6 43.6 %shard_map.211 = (bf16[64,512]{1,0:T(8,128)(2,1)S(1)}, f32[1024,64]{1,0:T(8,128)S(1)}, f32[1024,64]{1,0:T(8,128)S(1)}) custom-call(bf16[64,512]{1,0:T(8,128)(2,1)} %refs_0_.1, f32[4,1,512]{2,1,0:T(1,128)} %bitcast.28, f32[4,1,512]{2,1,0:T(1,128)} %bitcast.29, f32[16,64]{1,0:T(8,128)} %refs_3_.1, f32[16,64]{1,0:T(8,128)} %refs_4_.1, f32[1,16]{1,0:T(1,128)} %bitcast.33, ...), custom_call_target="tpu_custom_call" | custom-call | tf_op jit(solution)/shard_map/pallas_call | solution.py:624
  44.3 1.0 %shard_map.212 = (bf16[64,512]{1,0:T(8,128)(2,1)}, f32[1024,64]{1,0:T(8,128)}, f32[1024,64]{1,0:T(8,128)}) custom-call(bf16[64,512]{1,0:T(8,128)(2,1)S(1)} %get-tuple-element.9.refs_0_, f32[1024,64]{1,0:T(8,128)S(1)} %get-tuple-element.10.refs_1_, f32[1024,64]{1,0:T(8,128)S(1)} %get-tuple-element.11.refs_2_), custom_call_target="tpu_custom_call" | custom-call | tf_op jit(solution)/shard_map/pallas_call | solution.py:635

commit v3 on v2

--- a/solution.py
+++ b/solution.py
@@ -1,4 +1,5 @@
 import functools
+import math
 from types import SimpleNamespace
 
 import jax
@@ -138,11 +139,11 @@
     load_gates = [load(r.gate.at[0], r.gate_v), load(r.up.at[0], r.up_v)]
     load_down = load(r.down.at[0], r.down_v)
 
-    def remote(src, dst, send, recv, **where):
+    def remote(src, dst, recv, **where):
         return pltpu.make_async_remote_copy(
             src_ref=src,
             dst_ref=dst,
-            send_sem=send,
+            send_sem=r.sent.at[0],
             recv_sem=recv,
             device_id=where,
             device_id_type=pl.DeviceIdType.MESH,
@@ -155,14 +156,10 @@
         started.append(copy)
         return copy
 
+    def arrive(target, recv):
+        remote(target, target, recv, tp=tp_of[1]).wait_recv()
+
     load_tokens.wait()
-    pl.semaphore_wait(barrier, tp_count - 1 + ep_count - 1)
-    first = {
-        p: go(remote(r.pieces.at[0], r.pieces.at[p], r.a_send.at[p], r.a_recv.at[p],
-                     tp=tp_of[p]))
-        for p in (3, 1, 2)
-    }
-
     for copy in load_routes:
         copy.wait()
     choice, weight = r.choice_v[...], r.weight_v[...]
@@ -186,43 +183,45 @@
     r.table[...] = table.reshape(ep_count, capacity, row_count)
     r.out_tok[...] = dot(table, r.pieces[0]).astype(bf16).reshape(ep_count, capacity, width)
 
-    def spread(order, source, arrived, send, recv):
-        copies = {}
+    pl.semaphore_wait(barrier, tp_count - 1 + ep_count - 1)
+    first = {
+        p: go(remote(r.pieces.at[0], r.pieces.at[p], r.a_recv.at[p],
+                     tp=tp_of[p]))
+        for p in (3, 1, 2)
+    }
+
+    def spread(order, source, arrived, recv):
         for j in order:
-            copies[j] = go(remote(source.at[ep_of[j]], arrived.at[0, j], send.at[j], recv.at[j],
-                                  ep=ep_of[j]))
-        return copies
-
-    tok_z = spread(range(2, ep_count), r.out_tok, r.arr_tok, r.bz_send, r.bz_recv)
-    tok_near, tok_far, mix_near, mix_far = {}, {}, {}, {}
-
-    def forward(m, peers, z_copies, arrived, near, send, recv):
-        for j in (2 * m, 2 * m + 1):
-            z_copies[j].wait_recv()
+            go(remote(source.at[ep_of[j]], arrived.at[0, j], recv.at[j // 2], ep=ep_of[j]))
+
+    spread(range(2, ep_count), r.out_tok, r.arr_tok, r.bz_recv)
+    def forward(m, peers, arrived, z_recv, recv):
         block = pl.ds(2 * m, 2)
+        arrive(arrived.at[0, block], z_recv.at[m])
         for p in peers:
-            near[p, m] = go(remote(arrived.at[0, block], arrived.at[p, block], send.at[p, m],
-                                   recv.at[p, m], tp=tp_of[p]))
+            go(remote(arrived.at[0, block], arrived.at[p, block], recv[p], tp=tp_of[p]))
+
+    def side(m):
+        return 0 if m < pairs // 2 else 1
 
     def tok_forward(m):
-        forward(m, (1, 2), tok_z, r.arr_tok, tok_near, r.bn_send, r.bn_recv)
+        recv = {p: r.bn_recv.at[p - 1, m] for p in (1, 2)}
+        forward(m, (1, 2), r.arr_tok, r.bz_recv, recv)
 
     def tok_relay(m):
         for p in (1, 2):
-            tok_near[p, m].wait_recv()
+            arrive(r.arr_tok.at[p, pl.ds(2 * m, 2)], r.bn_recv.at[p - 1, m])
             j = 2 * m + p - 1
-            tok_far[p, m] = go(remote(r.arr_tok.at[p, j], r.arr_tok.at[3, j], r.bf_send.at[p, m],
-                                      r.bf_recv.at[p, m], tp=tp_of[3 - p]))
-
-    def share(pieces, shared, arrived, send, recv):
+            go(remote(r.arr_tok.at[p, j], r.arr_tok.at[3, j], r.bf_recv.at[side(m)],
+                      tp=tp_of[3 - p]))
+
+    def share(pieces, shared, arrived, recv):
         for p in range(tp_count):
             piece = pieces[p]
             arrived[p, 0] = dot(r.table[me_ep], piece).astype(bf16)
             shared[p] = dot(r.table[ep_of[1]], piece).astype(bf16)
-        return [
-            go(remote(shared.at[p], arrived.at[p, 1], send.at[p], recv.at[p], ep=ep_of[1]))
-            for p in range(tp_count)
-        ]
+        for p in range(tp_count):
+            go(remote(shared.at[p], arrived.at[p, 1], recv.at[0], ep=ep_of[1]))
 
     groups = r.decay.shape[0]
     entries = r.in_re_v.shape[1]
@@ -290,8 +289,6 @@
         drive = term if drive is None else drive + term
     drive = (drive * lax.rsqrt(squares / full + 1e-06)).astype(bf16)
 
-    for m in middle:
-        tok_forward(m)
     spread_drive = dot(r.replicate[...], drive).reshape(row_count, groups, channels)
     spread_drive = (spread_drive * r.own_group[...]).astype(bf16).reshape(rows, channels)
     push = dot(spread_drive, r.push_w[...])
@@ -306,8 +303,16 @@
     real, imag = r.state_rv[...], r.state_iv[...]
     next_real = wide_real * real - wide_imag * imag + push[:, :entries]
     next_imag = wide_real * imag + wide_imag * real + push[:, entries:]
-    r.next_r[...] = next_real
-    r.next_i[...] = next_imag
+    r.next_rv[...] = next_real
+    r.next_iv[...] = next_imag
+    kept = [
+        pltpu.make_async_copy(r.next_rv, r.next_r, r.out_sem.at[0]),
+        pltpu.make_async_copy(r.next_iv, r.next_i, r.out_sem.at[1]),
+    ]
+    for copy in kept:
+        copy.start()
+    for m in middle:
+        tok_forward(m)
     both = jnp.concatenate([next_real, next_imag], axis=1).astype(bf16)
     spread_y = dot(jnp.concatenate([both, both], axis=1), r.read_w[...])
     lane_group = lax.broadcasted_iota(jnp.int32, (row_count, 128), 1) // per_group
@@ -326,14 +331,15 @@
 
     r.out_mix[...] = dot(table, mixer).astype(bf16).reshape(ep_count, capacity, channels)
     far_first = [j for m in reversed(range(1, pairs)) for j in (2 * m, 2 * m + 1)]
-    mix_z = spread(far_first, r.out_mix, r.arr_mix, r.cz_send, r.cz_recv)
+    spread(far_first, r.out_mix, r.arr_mix, r.cz_recv)
     far_half = tuple(reversed(range(pairs // 2, pairs)))
     near_half = tuple(reversed(range(pairs // 2)))
     half = slots // 2
     blocks = ep_count // 2
 
     def mix_forward(m):
-        forward(m, (1, 2, 3), mix_z, r.arr_mix, mix_near, r.cn_send, r.cn_recv)
+        recv = {p: r.cn_recv.at[p - 1, side(m)] for p in (1, 2, 3)}
+        forward(m, (3, 1, 2), r.arr_mix, r.cz_recv, recv)
 
     for m in late:
         tok_forward(m)
@@ -343,18 +349,14 @@
     tok_relay(far_half[0])
     for m in far_half[1:]:
         mix_forward(m)
-    tok_share = share(r.pieces, r.shared_tok, r.arr_tok, r.bs_send, r.bs_recv)
+    share(r.pieces, r.shared_tok, r.arr_tok, r.bs_recv)
 
     def near_traffic():
-        copies = {
-            p: go(remote(r.mixers.at[0], r.mixers.at[p], r.e_send.at[p], r.e_recv.at[p],
-                         tp=tp_of[p]))
-            for p in (3, 1, 2)
-        }
+        for p in (3, 1, 2):
+            go(remote(r.mixers.at[0], r.mixers.at[p], r.e_recv.at[0], tp=tp_of[p]))
         for m in near_half[:-1]:
             tok_relay(m)
             mix_forward(m)
-        return copies
 
     mixed = r.mixed
 
@@ -362,41 +364,47 @@
         block = pl.ds(2 * chunk[-1], blocks)
         span = pl.ds(2 * chunk[-1] * capacity, half)
         remote_chunk = [m for m in chunk if m]
-        early = range(tp_count - 1) if chunk is far_half else ()
+        landed = pl.ds(2 * remote_chunk[-1], 2 * len(remote_chunk))
+        early = (0, 3) if chunk is far_half else ()
         for p in early:
             if p:
-                for m in remote_chunk:
-                    mix_near[p, m].wait_recv()
+                arrive(r.arr_mix.at[p, landed], r.cn_recv.at[p - 1, side(chunk[-1])])
             rows_of_p = r.arr_mix[p, block].reshape(half, channels)
             for n in range(tp_count):
                 columns = pl.ds(n * width, width)
                 term = dot(rows_of_p, r.w_out_v[tp_of[p], :, columns])
                 mixed[span, columns] = term if p == 0 else mixed[span, columns] + term
-        result = then() if then else None
-        for m in remote_chunk:
-            for p in (1, 2, 3):
-                if p == 3 or not early:
-                    mix_near[p, m].wait_recv()
-            for p in (1, 2):
-                tok_far[p, m].wait_recv()
+        if then:
+            then()
+        for p in (1, 2, 3):
+            if p not in early:
+                arrive(r.arr_mix.at[p, landed], r.cn_recv.at[p - 1, side(chunk[-1])])
+        arrive(r.arr_tok.at[3, landed], r.bf_recv.at[side(chunk[-1])])
         rest = [p for p in range(tp_count) if p not in early]
         squares = 0.0
+        if not early:
+            natural = jnp.concatenate(
+                [r.arr_mix[tp_of[n], block].reshape(half, channels) for n in range(tp_count)],
+                axis=1,
+            )
         for n in range(tp_count):
             columns = pl.ds(n * width, width)
-            term = mixed[span, columns] if early else 0.0
-            for p in rest:
-                rows_of_p = r.arr_mix[p, block].reshape(half, channels)
-                term = term + dot(rows_of_p, r.w_out_v[tp_of[p], :, columns])
+            if early:
+                term = mixed[span, columns]
+                for p in rest:
+                    rows_of_p = r.arr_mix[p, block].reshape(half, channels)
+                    term = term + dot(rows_of_p, r.w_out_v[tp_of[p], :, columns])
+            else:
+                term = dot(natural, r.w_out_v[:, :, columns].reshape(tp_count * channels, width))
             after = r.arr_tok[tp_of[n], block].reshape(half, width).astype(f32)
-            after = (after + term.astype(bf16).astype(f32)).astype(bf16).astype(f32)
+            after = after + term
             squares = squares + jnp.sum(after * after, axis=1, keepdims=True)
             r.normed[span, columns] = (after * r.gain_ffn_v[n]).astype(bf16)
         scale = lax.rsqrt(squares / full + 1e-06)
         r.scale[span] = jnp.broadcast_to(scale, (half, 128))
-        return result
 
     load_w_out.wait()
-    own_mix = mix_rows(far_half, near_traffic)
+    mix_rows(far_half, near_traffic)
     for copy in load_gates:
         copy.wait()
     load_down.wait()
@@ -418,80 +426,85 @@
         return pl.ds(j * capacity, capacity)
 
     parts, relay_in, parts_in, held = r.parts, r.relay_in, r.parts_in, r.held
-    far_send, pure_send, merged_send = {}, {}, {}
 
     def down(p, first):
         columns = pl.ds(pl.multiple_of(tp_of[p] * width, width), width)
         return dot(r.hidden[pl.ds(first, half)], r.down_v[:, columns])
 
-    def down_far(first, chunk):
-        parts[3, pl.ds(first, half)] = down(3, first).astype(bf16)
+    def share_mix():
+        arrive(r.mixers.at[pl.ds(1, tp_count - 1)], r.e_recv.at[0])
+        share(r.mixers, r.shared_mix, r.arr_mix, r.cs_recv)
+
+    def down_all(first, chunk, midway):
+        span = pl.ds(first, half)
+        for n in range(tp_count):
+            if n == tp_count // 2:
+                midway()
+            value = dot(r.hidden[span], r.down_v[:, pl.ds(n * width, width)])
+            held[n, span] = value
+            parts[n, span] = value.astype(bf16)
+        send_far(chunk)
+        for p in (1, 2):
+            send_pure(p, chunk)
+
+    def send_far(chunk):
         for m in chunk:
             for p in (1, 2):
                 j = 2 * m + p - 1
-                far_send[p, m] = go(remote(parts.at[3, rows_of(j)], relay_in.at[rows_of(j)],
-                                           r.rf_send.at[p, m], r.rf_recv.at[p, m], tp=tp_of[p]))
+                go(remote(parts.at[tp_of[3], rows_of(j)], relay_in.at[rows_of(j)],
+                          r.rf_recv.at[m], tp=tp_of[p]))
+
+    def send_pure(p, chunk):
+        for m in chunk:
+            j = 2 * m + p - 1
+            go(remote(parts.at[tp_of[p], rows_of(j)], parts_in.at[p, rows_of(j)],
+                      r.rs_recv.at[m], tp=tp_of[p]))
 
     def down_near(first, chunk):
-        for p in (1, 2):
-            value = down(p, first)
-            held[p, pl.ds(first, half)] = value
-            parts[p, pl.ds(first, half)] = value.astype(bf16)
-            for m in chunk:
-                j = 2 * m + p - 1
-                pure_send[p, m] = go(remote(parts.at[p, rows_of(j)], parts_in.at[p, rows_of(j)],
-                                            r.rp_send.at[p, m], r.rp_recv.at[p, m], tp=tp_of[p]))
+        span = pl.ds(first, half)
+        parts[tp_of[3], span] = down(3, first).astype(bf16)
+        send_far(chunk)
+        values = [down(p, first) for p in (1, 2)]
+        for p, value in zip((1, 2), values):
+            held[tp_of[p], span] = value
+            parts[tp_of[p], span] = value.astype(bf16)
+            send_pure(p, chunk)
 
     def down_own(first):
-        held[0, pl.ds(first, half)] = down(0, first)
+        held[tp_of[0], pl.ds(first, half)] = down(0, first)
 
     def merge(m):
+        arrive(relay_in.at[pl.ds(2 * m * capacity, 2 * capacity)], r.rf_recv.at[m])
         for p in (1, 2):
             q = 3 - p
             j = 2 * m + p - 1
-            far_send[p, m].wait_recv()
-            merged = held[q, rows_of(j)] + relay_in[rows_of(j)].astype(f32)
+            merged = held[tp_of[q], rows_of(j)] + relay_in[rows_of(j)].astype(f32)
             r.merged[rows_of(j)] = merged.astype(bf16)
-            merged_send[q, m] = go(remote(r.merged.at[rows_of(j)], parts_in.at[q, rows_of(j)],
-                                          r.rm_send.at[q, m], r.rm_recv.at[q, m], tp=tp_of[q]))
-
-    back = {}
+            go(remote(r.merged.at[rows_of(j)], parts_in.at[q, rows_of(j)], r.rs_recv.at[m],
+                      tp=tp_of[q]))
 
     def finish(m):
-        for p in (1, 2):
-            pure_send[p, m].wait_recv()
-            merged_send[p, m].wait_recv()
         span = pl.ds(2 * m * capacity, 2 * capacity)
-        total = held[0, span] + parts_in[1, span].astype(f32) + parts_in[2, span].astype(f32)
+        arrive(parts_in.at[pl.ds(1, 2), span], r.rs_recv.at[m])
+        total = held[tp_of[0], span] + parts_in[1, span].astype(f32) + parts_in[2, span].astype(f32)
         r.results[pl.ds(2 * m, 2)] = total.astype(bf16).reshape(2, capacity, width)
         for j in (2 * m + 1, 2 * m):
             if j:
-                back[j] = go(remote(r.results.at[j], r.returned.at[me_ep],
-                                    r.z_send.at[j], r.z_recv.at[j], ep=ep_of[j]))
+                go(remote(r.results.at[j], r.returned.at[me_ep], r.z_recv.at[0], ep=ep_of[j]))
 
     gate_up(half, 0, tiles)
-    for p in (1, 2, 3):
-        own_mix[p].wait_recv()
-    mix_share = share(r.mixers, r.shared_mix, r.arr_mix, r.cs_send, r.cs_recv)
-    down_far(half, far_half)
-    down_near(half, far_half)
-    down_own(half)
-    for copy in tok_share + mix_share:
-        copy.wait_recv()
+    down_all(half, far_half, share_mix)
+    arrive(r.arr_tok.at[:, 1], r.bs_recv.at[0])
+    arrive(r.arr_mix.at[:, 1], r.cs_recv.at[0])
     mix_rows(near_half)
     gate_up(0, 0, tiles // 2)
     for m in far_half:
         merge(m)
     gate_up(0, tiles // 2, tiles)
-    down_far(0, near_half)
     down_near(0, near_half)
     for m in far_half:
         finish(m)
     down_own(0)
-    for m in near_half:
-        merge(m)
-    for m in near_half[:-1]:
-        finish(m)
     own = pl.ds(pl.multiple_of(me_tp * width, width), width)
     mixed_own = None
     for p in range(tp_count):
@@ -500,16 +513,23 @@
     after_own = (
         (r.pieces[0].astype(f32) + mixed_own.astype(bf16).astype(f32)).astype(bf16).astype(f32)
     )
+    for m in near_half:
+        merge(m)
+    for m in near_half[:-1]:
+        finish(m)
     finish(0)
     r.returned[me_ep] = r.results[0]
-    for j in range(1, ep_count):
-        remote(r.results.at[j], r.returned.at[ep_of[j]], r.z_send.at[j],
-               r.z_recv.at[j], ep=ep_of[j]).wait_recv()
+    arrive(r.results.at[pl.ds(1, ep_count - 1)], r.z_recv.at[0])
     everything = r.returned[...].reshape(slots, width)
     weighted = dot(r.combine[0], everything) + dot(r.combine[1], everything)
-    r.out[...] = (after_own + weighted).astype(bf16)
-    for copy in started:
-        copy.wait_send()
+    r.out_v[...] = (after_own + weighted).astype(bf16)
+    kept.append(pltpu.make_async_copy(r.out_v, r.out, r.out_sem.at[2]))
+    kept[-1].start()
+    total = sum(2 * math.prod(copy.src_ref.shape) for copy in started)
+    sent = r.gate_v.at[pl.ds(0, total // (2 * hidden_width))]
+    remote(sent, sent, r.a_recv.at[0], tp=tp_of[1]).wait_send()
+    for copy in kept:
+        copy.wait()
 
 
 def write_kernel(*refs):
@@ -605,27 +625,31 @@
         normed=pltpu.VMEM((slots, full), bf16),
         hidden=pltpu.VMEM((slots, hidden_width), bf16),
         parts=pltpu.VMEM((tp_count, slots, width), bf16),
-        held=pltpu.VMEM((3, slots, width), f32),
+        held=pltpu.VMEM((tp_count, slots, width), f32),
         relay_in=pltpu.VMEM((slots, width), bf16),
         merged=pltpu.VMEM((slots, width), bf16),
         parts_in=pltpu.VMEM((3, slots, width), bf16),
         results=pltpu.VMEM((ep_count, capacity, width), bf16),
         returned=pltpu.VMEM((ep_count, capacity, width), bf16),
         load_sem=dma(20),
+        out_sem=dma(3),
+        next_rv=pltpu.VMEM((rows, entries), f32),
+        next_iv=pltpu.VMEM((rows, entries), f32),
+        out_v=pltpu.VMEM((row_count, width), bf16),
     )
     kinds = dict(
-        a=(tp_count,), e=(tp_count,), bs=(tp_count,), cs=(tp_count,), bz=(ep_count,), cz=(ep_count,), z=(ep_count,),
-        bn=(3, pairs), bf=(3, pairs), cn=(4, pairs),
-        rf=(3, pairs), rp=(3, pairs), rm=(3, pairs),
+        sent=(1,), a_recv=(tp_count,), e_recv=(1,), bs_recv=(1,), cs_recv=(1,), z_recv=(1,),
+        bz_recv=(pairs,), cz_recv=(pairs,), bn_recv=(2, pairs), bf_recv=(2,), cn_recv=(3, 2),
+        rf_recv=(pairs,), rs_recv=(pairs,),
     )
     for name, shape in kinds.items():
-        scratch[name + "_send"], scratch[name + "_recv"] = dma(*shape), dma(*shape)
+        scratch[name] = dma(*shape)
     names = (tuple(inputs), tuple(outputs), tuple(scratch))
     out, next_real, next_imag = pl.pallas_call(
         functools.partial(layer_kernel, ep_count, tp_count, names),
         out_shape=tuple(outputs.values()),
         in_specs=[spec for _, spec in inputs.values()],
-        out_specs=(vmem, vmem, vmem),
+        out_specs=(hbm, hbm, hbm),
         scratch_shapes=list(scratch.values()),
         compiler_params=pltpu.CompilerParams(
             collective_id=0, has_side_effects=True, vmem_limit_bytes=60 * 1024 * 1024
@@ -635,7 +659,7 @@
     out, next_real, next_imag = pl.pallas_call(
         write_kernel,
         out_shape=tuple(jax.ShapeDtypeStruct(x.shape, x.dtype) for x in results),
-        in_specs=[vmem] * 3,
+        in_specs=[hbm] * 3,
         out_specs=(hbm, hbm, hbm),
         scratch_shapes=[dma(3)],
     )(*results)

time: 45.4 us -> 43.7 us (0.963)
  Pallas kernels: 44.6 us -> 42.9 us
    pallas_call x1, Pallas kernels: 43.6 us -> 41.9 us  [layer_call(): pl.pallas_call(functools.partial(layer_kernel, ep_count, tp_count, names)...]
where the time goes in v3:
time: 43.7 us; the launch traced here: 43.6 us
  Pallas kernels  42.9 us (98%)
  between operations  0.65 us (1%)
    pallas_call x1, Pallas kernels, layer_call(): pl.pallas_call(functools.partial(layer_kernel, ep_count, tp_count, names)...  41.9 us
    pallas_call x1, Pallas kernels, layer_call(): pl.pallas_call(write_kernel, out_shape=tuple((jax.ShapeDtypeStruct(x.shap...  1.02 us

profile of v3, /device:TPU:0, one launch (start us, length us, event | category | flops | bytes accessed | tf_op | source)
XLA Modules:
  0.0 43.6 jit_solution(8454246972885523409)
XLA Ops:
  0.6 41.9 %shard_map.211 = (bf16[64,512]{1,0:T(8,128)(2,1)S(1)}, f32[1024,64]{1,0:T(8,128)S(1)}, f32[1024,64]{1,0:T(8,128)S(1)}) custom-call(bf16[64,512]{1,0:T(8,128)(2,1)} %refs_0_.1, f32[4,1,512]{2,1,0:T(1,128)} %bitcast.28, f32[4,1,512]{2,1,0:T(1,128)} %bitcast.29, f32[16,64]{1,0:T(8,128)} %refs_3_.1, f32[16,64]{1,0:T(8,128)} %refs_4_.1, f32[1,16]{1,0:T(1,128)} %bitcast.33, ...), custom_call_target="tpu_custom_call" | custom-call | tf_op jit(solution)/shard_map/pallas_call | solution.py:648
  42.5 1.0 %shard_map.212 = (bf16[64,512]{1,0:T(8,128)(2,1)}, f32[1024,64]{1,0:T(8,128)}, f32[1024,64]{1,0:T(8,128)}) custom-call(bf16[64,512]{1,0:T(8,128)(2,1)S(1)} %get-tuple-element.9.refs_0_, f32[1024,64]{1,0:T(8,128)S(1)} %get-tuple-element.10.refs_1_, f32[1024,64]{1,0:T(8,128)S(1)} %get-tuple-element.11.refs_2_), custom_call_target="tpu_custom_call" | custom-call | tf_op jit(solution)/shard_map/pallas_call | solution.py:659

commit v4 on v3

--- a/solution.py
+++ b/solution.py
@@ -112,32 +112,34 @@
 
     loads = []
 
-    def load(source, target):
-        loads.append(pltpu.make_async_copy(source, target, r.load_sem.at[len(loads)]))
-        loads[-1].start()
-        return loads[-1]
-
-    load_tokens = load(r.tokens, r.pieces.at[0])
-    load_routes = [load(r.choice, r.choice_v), load(r.weight, r.weight_v)]
-    load_small = [
-        load(r.decay, r.decay_v),
-        load(r.freq, r.freq_v),
-        load(r.step, r.step_v),
-        load(r.pass_, r.pass_v),
-        load(r.gain_mix, r.gain_mix_v),
-        load(r.gain_ffn, r.gain_ffn_v),
-    ]
-    load_mats = [
-        load(r.in_re, r.in_re_v),
-        load(r.in_im, r.in_im_v),
-        load(r.re_re, r.re_re_v),
-        load(r.re_im, r.re_im_v),
-    ]
-    load_w_in = load(r.w_in, r.w_in_v)
-    load_states = [load(r.state_r, r.state_rv), load(r.state_i, r.state_iv)]
-    load_w_out = load(r.w_out, r.w_out_v)
-    load_gates = [load(r.gate.at[0], r.gate_v), load(r.up.at[0], r.up_v)]
-    load_down = load(r.down.at[0], r.down_v)
+    def load(*pairs):
+        sem = r.load_sem.at[len(loads)]
+        for source, target in pairs:
+            pltpu.make_async_copy(source, target, sem).start()
+        loads.append(sem)
+        return sem
+
+    def loaded(target, sem):
+        pltpu.make_async_copy(target, target, sem).wait()
+
+    load_tokens = load((r.tokens, r.pieces.at[0]))
+    load_choice = load((r.choice, r.choice_v))
+    load_weight = load((r.weight, r.weight_v))
+    load_poles = load((r.decay, r.poles_v.at[0]), (r.freq, r.poles_v.at[1]))
+    load_step = load((r.step, r.step_v))
+    load_pass = load((r.pass_, r.pass_v))
+    load_gains = load((r.gain_mix, r.gains_v.at[0]), (r.gain_ffn, r.gains_v.at[1]))
+    load_mats = load(
+        (r.in_re, r.mats_v.at[0]),
+        (r.in_im, r.mats_v.at[1]),
+        (r.re_re, r.mats_v.at[2]),
+        (r.re_im, r.mats_v.at[3]),
+    )
+    load_w_in = load((r.w_in, r.w_in_v))
+    load_states = load((r.state_r, r.states_v.at[0]), (r.state_i, r.states_v.at[1]))
+    load_w_out = load((r.w_out, r.w_out_v))
+    load_gates = load((r.gate.at[0], r.gates_v.at[0]), (r.up.at[0], r.gates_v.at[1]))
+    load_down = load((r.down.at[0], r.down_v))
 
     def remote(src, dst, recv, **where):
         return pltpu.make_async_remote_copy(
@@ -159,9 +161,9 @@
     def arrive(target, recv):
         remote(target, target, recv, tp=tp_of[1]).wait_recv()
 
-    load_tokens.wait()
-    for copy in load_routes:
-        copy.wait()
+    loaded(r.pieces.at[0], load_tokens)
+    loaded(r.choice_v, load_choice)
+    loaded(r.weight_v, load_weight)
     choice, weight = r.choice_v[...], r.weight_v[...]
     top_count = choice.shape[0]
     experts = lax.broadcasted_iota(jnp.int32, (ep_count, row_count), 0)
@@ -224,17 +226,19 @@
             go(remote(shared.at[p], arrived.at[p, 1], recv.at[0], ep=ep_of[1]))
 
     groups = r.decay.shape[0]
-    entries = r.in_re_v.shape[1]
+    entries = r.mats_v.shape[2]
     per_group = channels // groups
     eye = (
         lax.broadcasted_iota(jnp.int32, (groups, groups), 0)
         == lax.broadcasted_iota(jnp.int32, (groups, groups), 1)
     ).astype(f32)
-    for copy in load_small:
-        copy.wait()
+    loaded(r.poles_v, load_poles)
+    loaded(r.step_v, load_step)
+    loaded(r.pass_v, load_pass)
+    loaded(r.gains_v, load_gains)
     step = jnp.sum(eye * jnp.exp(r.step_v[...]), axis=1, keepdims=True)
-    lam = -r.decay_v[...]
-    frequency = r.freq_v[...]
+    lam = -r.poles_v[0]
+    frequency = r.poles_v[1]
     magnitude = jnp.exp(lam * step)
     abar_real = magnitude * jnp.cos(frequency * step)
     abar_imag = magnitude * jnp.sin(frequency * step)
@@ -249,15 +253,14 @@
         )
 
     wide_real, wide_imag = per_channel(factor_real), per_channel(factor_imag)
-    for copy in load_mats:
-        copy.wait()
-    in_re, in_im = r.in_re_v[...], r.in_im_v[...]
+    loaded(r.mats_v, load_mats)
+    in_re, in_im = r.mats_v[0], r.mats_v[1]
     push_w = jnp.concatenate(
         [wide_real * in_re - wide_imag * in_im, wide_real * in_im + wide_imag * in_re], axis=1
     )
     push_high, push_low = halves(push_w)
     r.push_w[...] = jnp.concatenate([push_high, push_low], axis=1)
-    read_w = jnp.concatenate([r.re_re_v[...], -r.re_im_v[...]], axis=1).T
+    read_w = jnp.concatenate([r.mats_v[2], -r.mats_v[3]], axis=1).T
     read_high, read_low = halves(read_w)
     r.read_w[...] = jnp.concatenate([read_high, read_low], axis=0)
     weight_high, weight_low = halves(weights.T)
@@ -284,8 +287,8 @@
         piece = r.pieces[p].astype(f32)
         squares = squares + jnp.sum(piece * piece, axis=1, keepdims=True)
         if not p:
-            load_w_in.wait()
-        term = dot((piece * r.gain_mix_v[tp_of[p]]).astype(bf16), r.w_in_v[tp_of[p]])
+            loaded(r.w_in_v, load_w_in)
+        term = dot((piece * r.gains_v[0, tp_of[p]]).astype(bf16), r.w_in_v[tp_of[p]])
         drive = term if drive is None else drive + term
     drive = (drive * lax.rsqrt(squares / full + 1e-06)).astype(bf16)
 
@@ -293,14 +296,13 @@
     spread_drive = (spread_drive * r.own_group[...]).astype(bf16).reshape(rows, channels)
     push = dot(spread_drive, r.push_w[...])
     push = push[:, : 2 * entries] + push[:, 2 * entries :]
-    for copy in load_states:
-        copy.wait()
+    loaded(r.states_v, load_states)
 
     def per_row(values):
         return jnp.broadcast_to(values[None], (row_count, groups, entries)).reshape(rows, entries)
 
     wide_real, wide_imag = per_row(r.abar[0]), per_row(r.abar[1])
-    real, imag = r.state_rv[...], r.state_iv[...]
+    real, imag = r.states_v[0], r.states_v[1]
     next_real = wide_real * real - wide_imag * imag + push[:, :entries]
     next_imag = wide_real * imag + wide_imag * real + push[:, entries:]
     r.next_rv[...] = next_real
@@ -399,15 +401,14 @@
             after = r.arr_tok[tp_of[n], block].reshape(half, width).astype(f32)
             after = after + term
             squares = squares + jnp.sum(after * after, axis=1, keepdims=True)
-            r.normed[span, columns] = (after * r.gain_ffn_v[n]).astype(bf16)
+            r.normed[span, columns] = (after * r.gains_v[1, n]).astype(bf16)
         scale = lax.rsqrt(squares / full + 1e-06)
         r.scale[span] = jnp.broadcast_to(scale, (half, 128))
 
-    load_w_out.wait()
+    loaded(r.w_out_v, load_w_out)
     mix_rows(far_half, near_traffic)
-    for copy in load_gates:
-        copy.wait()
-    load_down.wait()
+    loaded(r.gates_v, load_gates)
+    loaded(r.down_v, load_down)
     hidden_width = r.hidden.shape[1]
     tile = next(t for t in (512, 256, 128) if hidden_width % t == 0)
     tiles = hidden_width // tile
@@ -418,8 +419,8 @@
         for n in range(start, stop):
             columns = pl.ds(n * tile, tile)
             scale = r.scale[span, :1]
-            gate = dot(r.normed[span], r.gate_v[:, columns]) * scale
-            upper = dot(r.normed[span], r.up_v[:, columns]) * scale
+            gate = dot(r.normed[span], r.gates_v[0, :, columns]) * scale
+            upper = dot(r.normed[span], r.gates_v[1, :, columns]) * scale
             r.hidden[span, columns] = (jax.nn.silu(gate) * upper).astype(bf16)
 
     def rows_of(j):
@@ -434,18 +435,6 @@
     def share_mix():
         arrive(r.mixers.at[pl.ds(1, tp_count - 1)], r.e_recv.at[0])
         share(r.mixers, r.shared_mix, r.arr_mix, r.cs_recv)
-
-    def down_all(first, chunk, midway):
-        span = pl.ds(first, half)
-        for n in range(tp_count):
-            if n == tp_count // 2:
-                midway()
-            value = dot(r.hidden[span], r.down_v[:, pl.ds(n * width, width)])
-            held[n, span] = value
-            parts[n, span] = value.astype(bf16)
-        send_far(chunk)
-        for p in (1, 2):
-            send_pure(p, chunk)
 
     def send_far(chunk):
         for m in chunk:
@@ -460,10 +449,12 @@
             go(remote(parts.at[tp_of[p], rows_of(j)], parts_in.at[p, rows_of(j)],
                       r.rs_recv.at[m], tp=tp_of[p]))
 
+    def down_far(first, chunk):
+        parts[tp_of[3], pl.ds(first, half)] = down(3, first).astype(bf16)
+        send_far(chunk)
+
     def down_near(first, chunk):
         span = pl.ds(first, half)
-        parts[tp_of[3], span] = down(3, first).astype(bf16)
-        send_far(chunk)
         values = [down(p, first) for p in (1, 2)]
         for p, value in zip((1, 2), values):
             held[tp_of[p], span] = value
@@ -493,7 +484,10 @@
                 go(remote(r.results.at[j], r.returned.at[me_ep], r.z_recv.at[0], ep=ep_of[j]))
 
     gate_up(half, 0, tiles)
-    down_all(half, far_half, share_mix)
+    down_far(half, far_half)
+    down_near(half, far_half)
+    share_mix()
+    down_own(half)
     arrive(r.arr_tok.at[:, 1], r.bs_recv.at[0])
     arrive(r.arr_mix.at[:, 1], r.cs_recv.at[0])
     mix_rows(near_half)
@@ -501,8 +495,10 @@
     for m in far_half:
         merge(m)
     gate_up(0, tiles // 2, tiles)
+    down_far(0, near_half)
+    finish(far_half[0])
     down_near(0, near_half)
-    for m in far_half:
+    for m in far_half[1:]:
         finish(m)
     down_own(0)
     own = pl.ds(pl.multiple_of(me_tp * width, width), width)
@@ -522,11 +518,9 @@
     arrive(r.results.at[pl.ds(1, ep_count - 1)], r.z_recv.at[0])
     everything = r.returned[...].reshape(slots, width)
     weighted = dot(r.combine[0], everything) + dot(r.combine[1], everything)
-    r.out_v[...] = (after_own + weighted).astype(bf16)
-    kept.append(pltpu.make_async_copy(r.out_v, r.out, r.out_sem.at[2]))
-    kept[-1].start()
+    r.out[...] = (after_own + weighted).astype(bf16)
     total = sum(2 * math.prod(copy.src_ref.shape) for copy in started)
-    sent = r.gate_v.at[pl.ds(0, total // (2 * hidden_width))]
+    sent = r.gates_v.at[0, pl.ds(0, total // (2 * hidden_width))]
     remote(sent, sent, r.a_recv.at[0], tp=tp_of[1]).wait_send()
     for copy in kept:
         copy.wait()
@@ -588,12 +582,13 @@
         pieces=pltpu.VMEM((tp_count, row_count, width), bf16),
         choice_v=pltpu.VMEM(expert_choice.shape[::-1], expert_choice.dtype),
         weight_v=pltpu.VMEM(expert_weight.shape[::-1], f32),
-        decay_v=pltpu.VMEM((groups, entries), f32),
-        freq_v=pltpu.VMEM((groups, entries), f32),
+        poles_v=pltpu.VMEM((2, groups, entries), f32),
+        gains_v=pltpu.VMEM((2, tp_count, 1, width), f32),
+        mats_v=pltpu.VMEM((4, channels, entries), f32),
+        states_v=pltpu.VMEM((2, rows, entries), f32),
+        gates_v=pltpu.VMEM((2, full, hidden_width), bf16),
         step_v=pltpu.VMEM((1, groups), f32),
         pass_v=pltpu.VMEM((1, channels), f32),
-        gain_mix_v=pltpu.VMEM((tp_count, 1, width), f32),
-        gain_ffn_v=pltpu.VMEM((tp_count, 1, width), f32),
         table=pltpu.VMEM((ep_count, capacity, row_count), bf16),
         replicate=pltpu.VMEM((rows, row_count), bf16),
         own_group=pltpu.VMEM((groups, channels), f32),
@@ -601,16 +596,8 @@
         shared_tok=pltpu.VMEM((tp_count, capacity, width), bf16),
         shared_mix=pltpu.VMEM((tp_count, capacity, channels), bf16),
         scale=pltpu.VMEM((slots, 128), f32),
-        in_re_v=pltpu.VMEM((channels, entries), f32),
-        in_im_v=pltpu.VMEM((channels, entries), f32),
-        re_re_v=pltpu.VMEM((channels, entries), f32),
-        re_im_v=pltpu.VMEM((channels, entries), f32),
-        state_rv=pltpu.VMEM((rows, entries), f32),
-        state_iv=pltpu.VMEM((rows, entries), f32),
         w_in_v=pltpu.VMEM((tp_count, width, channels), bf16),
         w_out_v=pltpu.VMEM((tp_count, channels, full), bf16),
-        gate_v=pltpu.VMEM((full, hidden_width), bf16),
-        up_v=pltpu.VMEM((full, hidden_width), bf16),
         down_v=pltpu.VMEM((hidden_width, full), bf16),
         push_w=pltpu.VMEM((channels, 4 * entries), bf16),
         read_w=pltpu.VMEM((4 * entries, channels), bf16),
@@ -631,11 +618,10 @@
         parts_in=pltpu.VMEM((3, slots, width), bf16),
         results=pltpu.VMEM((ep_count, capacity, width), bf16),
         returned=pltpu.VMEM((ep_count, capacity, width), bf16),
-        load_sem=dma(20),
-        out_sem=dma(3),
+        load_sem=dma(13),
+        out_sem=dma(2),
         next_rv=pltpu.VMEM((rows, entries), f32),
         next_iv=pltpu.VMEM((rows, entries), f32),
-        out_v=pltpu.VMEM((row_count, width), bf16),
     )
     kinds = dict(
         sent=(1,), a_recv=(tp_count,), e_recv=(1,), bs_recv=(1,), cs_recv=(1,), z_recv=(1,),
@@ -649,7 +635,7 @@
         functools.partial(layer_kernel, ep_count, tp_count, names),
         out_shape=tuple(outputs.values()),
         in_specs=[spec for _, spec in inputs.values()],
-        out_specs=(hbm, hbm, hbm),
+        out_specs=(vmem, hbm, hbm),
         scratch_shapes=list(scratch.values()),
         compiler_params=pltpu.CompilerParams(
             collective_id=0, has_side_effects=True, vmem_limit_bytes=60 * 1024 * 1024

time: 43.7 us -> 43.1 us (0.986)
  Pallas kernels: 42.9 us -> 42.3 us
    pallas_call x1, Pallas kernels: 41.9 us -> 41.3 us  [layer_call(): pl.pallas_call(functools.partial(layer_kernel, ep_count, tp_count, names)...]
where the time goes in v4:
time: 43.1 us; the launch traced here: 42.9 us
  Pallas kernels  42.3 us (98%)
  between operations  0.65 us (2%)
    pallas_call x1, Pallas kernels, layer_call(): pl.pallas_call(functools.partial(layer_kernel, ep_count, tp_count, names)...  41.3 us
    pallas_call x1, Pallas kernels, layer_call(): pl.pallas_call(write_kernel, out_shape=tuple((jax.ShapeDtypeStruct(x.shap...  1.02 us

profile of v4, /device:TPU:0, one launch (start us, length us, event | category | flops | bytes accessed | tf_op | source)
XLA Modules:
  0.0 42.9 jit_solution(16166068467047198022)
XLA Ops:
  0.6 41.3 %shard_map.211 = (bf16[64,512]{1,0:T(8,128)(2,1)S(1)}, f32[1024,64]{1,0:T(8,128)S(1)}, f32[1024,64]{1,0:T(8,128)S(1)}) custom-call(bf16[64,512]{1,0:T(8,128)(2,1)} %refs_0_.1, f32[4,1,512]{2,1,0:T(1,128)} %bitcast.28, f32[4,1,512]{2,1,0:T(1,128)} %bitcast.29, f32[16,64]{1,0:T(8,128)} %refs_3_.1, f32[16,64]{1,0:T(8,128)} %refs_4_.1, f32[1,16]{1,0:T(1,128)} %bitcast.33, ...), custom_call_target="tpu_custom_call" | custom-call | tf_op jit(solution)/shard_map/pallas_call | solution.py:634
  41.9 1.0 %shard_map.212 = (bf16[64,512]{1,0:T(8,128)(2,1)}, f32[1024,64]{1,0:T(8,128)}, f32[1024,64]{1,0:T(8,128)}) custom-call(bf16[64,512]{1,0:T(8,128)(2,1)S(1)} %get-tuple-element.9.refs_0_, f32[1024,64]{1,0:T(8,128)S(1)} %get-tuple-element.10.refs_1_, f32[1024,64]{1,0:T(8,128)S(1)} %get-tuple-element.11.refs_2_), custom_call_target="tpu_custom_call" | custom-call | tf_op jit(solution)/shard_map/pallas_call | solution.py:645

commit v5 on v4

--- a/solution.py
+++ b/solution.py
@@ -410,7 +410,7 @@
     loaded(r.gates_v, load_gates)
     loaded(r.down_v, load_down)
     hidden_width = r.hidden.shape[1]
-    tile = next(t for t in (512, 256, 128) if hidden_width % t == 0)
+    tile = next(t for t in (1024, 512, 256, 128) if hidden_width % t == 0)
     tiles = hidden_width // tile
 
     def gate_up(first, start, stop):

time: 43.1 us -> 43.1 us (level)
  no operation moved by 1% of the time
where the time goes in v5:
time: 43.1 us; the launch traced here: 42.9 us
  Pallas kernels  42.3 us (98%)
  between operations  0.65 us (2%)
    pallas_call x1, Pallas kernels, layer_call(): pl.pallas_call(functools.partial(layer_kernel, ep_count, tp_count, names)...  41.3 us
    pallas_call x1, Pallas kernels, layer_call(): pl.pallas_call(write_kernel, out_shape=tuple((jax.ShapeDtypeStruct(x.shap...  1.02 us

profile of v5, /device:TPU:0, one launch (start us, length us, event | category | flops | bytes accessed | tf_op | source)
XLA Modules:
  0.0 42.9 jit_solution(6407398340054913322)
XLA Ops:
  0.6 41.3 %shard_map.211 = (bf16[64,512]{1,0:T(8,128)(2,1)S(1)}, f32[1024,64]{1,0:T(8,128)S(1)}, f32[1024,64]{1,0:T(8,128)S(1)}) custom-call(bf16[64,512]{1,0:T(8,128)(2,1)} %refs_0_.1, f32[4,1,512]{2,1,0:T(1,128)} %bitcast.28, f32[4,1,512]{2,1,0:T(1,128)} %bitcast.29, f32[16,64]{1,0:T(8,128)} %refs_3_.1, f32[16,64]{1,0:T(8,128)} %refs_4_.1, f32[1,16]{1,0:T(1,128)} %bitcast.33, ...), custom_call_target="tpu_custom_call" | custom-call | tf_op jit(solution)/shard_map/pallas_call | solution.py:634
  41.9 1.0 %shard_map.212 = (bf16[64,512]{1,0:T(8,128)(2,1)}, f32[1024,64]{1,0:T(8,128)}, f32[1024,64]{1,0:T(8,128)}) custom-call(bf16[64,512]{1,0:T(8,128)(2,1)S(1)} %get-tuple-element.9.refs_0_, f32[1024,64]{1,0:T(8,128)S(1)} %get-tuple-element.10.refs_1_, f32[1024,64]{1,0:T(8,128)S(1)} %get-tuple-element.11.refs_2_), custom_call_target="tpu_custom_call" | custom-call | tf_op jit(solution)/shard_map/pallas_call | solution.py:645
